TPU v7x, 32 devices: a whole 2x2x4 slice. The times are simulated.
32 devices in a mesh: sp: 8 (over z, y), tp: 4 (over x, core).
Axes of the slice: x: 2, y: 2, z: 4, core: 2. Of those that a mesh axis runs over, the one named last changes fastest.
Arguments:
- resid: bfloat16 [2048, 2048], P(('sp', 'tp')), may hold values from -0.3125 to 0.3125
- q_latent: bfloat16 [2048, 768], P('sp'), may hold values from -6 to 6
- kv_latent: bfloat16 [2048, 512], P('sp'), may hold values from -6 to 6
- rope_key: bfloat16 [2048, 32], P('sp'), may hold values from -6 to 6
- q_gain: float32 [768], replicated, may hold values from 0.6 to 10, as said below
- kv_gain: float32 [512], replicated, may hold values from 0.6 to 10
- w_q_small: bfloat16 [768, 768], P(None, 'tp'), may hold values from -0.21875 to 0.21875
- w_q_large: bfloat16 [768, 1280], P(None, 'tp'), may hold values from -0.21875 to 0.21875
- w_kv_small: bfloat16 [512, 1024], P(None, 'tp'), may hold values from -0.25 to 0.25
- w_kv_large: bfloat16 [512, 2048], P(None, 'tp'), may hold values from -0.25 to 0.25
- w_out_small: bfloat16 [512, 2048], P('tp'), may hold values from -0.15625 to 0.15625
- w_out_large: bfloat16 [1024, 2048], P('tp'), may hold values from -0.15625 to 0.15625
- ffn_gain: float32 [2048], replicated, may hold values from 0.1 to 1.9
- w_up: bfloat16 [2048, 8192], P('sp', 'tp'), may hold values from -0.125 to 0.125
- w_down: bfloat16 [8192, 2048], P('tp', 'sp'), may hold values from -0.0625 to 0.0625
Outputs:
- layer_out: bfloat16 [2048, 2048], P(('sp', 'tp'))
Inputs may be any that keep to these rules, and one draw needn't show every extreme that they name: q_gain and kv_gain are positive.
All inputs are finite; a program needn't handle non-finite values.
Results may differ from a plain program's by a relative error of at most 0.025.
The roundings to bfloat16 on the way count: a program that leaves them out, or rounds other values in their place, can miss the bound.
Values may be sent and summed in bfloat16 or wider, within the bound.
A program may use at most 128 MiB of HBM per device.

v0:
```python
import functools

import jax
import jax.numpy as jnp
from jax import lax
from jax.experimental import pallas as pl
from jax.experimental.pallas import tpu as pltpu
from jax.sharding import PartitionSpec as P

SMALL_DIM = 64
LARGE_DIM = 128
ROPE_DIM = 32


epsilon = 1e-06
theta_base = 10000.0
mask_floor = -1e30


def rms_scale(inputs, gain_vec):
    values = inputs.astype(jnp.float32)
    return (
        values * lax.rsqrt(jnp.mean(values * values, axis=-1, keepdims=True) + epsilon) * gain_vec
    )


def rotary(values, positions):
    halfway = values.shape[-1] // 2
    inverse = theta_base ** (-jnp.arange(0, 2 * halfway, 2, dtype=jnp.float32) / (2 * halfway))
    angles = positions.astype(jnp.float32)[:, None] * inverse[None, :]
    cos_table = jnp.cos(angles)
    sin_table = jnp.sin(angles)
    if values.ndim == 3:
        cos_table = cos_table[:, None, :]
        sin_table = sin_table[:, None, :]
    first_half = values[..., :halfway]
    second_half = values[..., halfway:]
    return jnp.concatenate(
        [
            first_half * cos_table - second_half * sin_table,
            second_half * cos_table + first_half * sin_table,
        ],
        axis=-1,
    )


def queries(normed, weight, nope_dim, positions):
    projected = jnp.dot(normed, weight, preferred_element_type=jnp.float32)
    projected = projected.reshape(projected.shape[0], -1, nope_dim + ROPE_DIM)
    turned = rotary(projected[..., nope_dim:], positions)
    return jnp.concatenate([projected[..., :nope_dim], turned], axis=-1).astype(jnp.bfloat16)


MESH = pl.DeviceIdType.MESH
CORES = 2
LANES = 128


def inner_split(count):
    best = 1
    for size in range(1, count + 1):
        if size * size <= count and count % size == 0:
            best = size
    return best


def remote(src, dst, send_sem, recv_sem, device):
    return pltpu.make_async_remote_copy(
        src_ref=src,
        dst_ref=dst,
        send_sem=send_sem,
        recv_sem=recv_sem,
        device_id=device,
        device_id_type=MESH,
    )


def place(ny, nz, nx):
    s, t = lax.axis_index("sp"), lax.axis_index("tp")
    z, y = s // ny, s % ny
    x, c = t // CORES, t % CORES

    def at(zz, yy, xx, cc):
        return (zz * ny + yy, xx * CORES + cc)

    return z, y, x, c, at


def greet(devices):
    barrier = pltpu.get_barrier_semaphore()
    for device in devices:
        pl.semaphore_signal(barrier, inc=1, device_id=device, device_id_type=MESH)
    pl.semaphore_wait(barrier, len(devices))


def layer_kernel(
    ny, nz, nx, lat_ref, q_ref, wks_ref, wkl_ref, wos_ref, wol_ref, resid_ref, gain_ref, up_ref,
    dn_ref, out_ref, lat_out, up_out, dn_out, row_max, row_sum, weighted, part_ref,
    rs_in, after, xg, pbuf, cbuf, xbuf, zsend, zbuf, own_sem,
    lz_s, lz_r, ly_s, ly_r, lc_s, lc_r, uz_s, uz_r, uy_s, uy_r, dz_s, dz_r, dy_s, dy_r,
    a_s, a_r, bz_s, bz_r, bx_s, bx_r, bc_s, bc_r, cc_s, cc_r, cx_s, cx_r, cz_s, cz_r,
):
    z, y, x, c, at = place(ny, nz, nx)
    s = z * ny + y
    rows = lat_ref.shape[0]
    half = rows // CORES
    units = up_out.shape[2]
    tp = nx * CORES
    t = x * CORES + c
    mine = pl.ds(pl.multiple_of(c * half, half), half)
    other = pl.ds(pl.multiple_of((1 - c) * half, half), half)
    partner = at(z, y, x, 1 - c)
    zdev = [at((z + k) % nz, y, x, c) for k in range(nz)]
    ydev = [at(z, (y + j) % ny, x, c) for j in range(ny)]
    zback = [at((z - k + nz) % nz, y, x, c) for k in range(nz)]
    xdev = [at(z, y, (x + j) % nx, c) for j in range(nx)]
    tdev = [(s, (t + k) % tp) for k in range(tp)]
    greet(zdev[1:] + ydev[1:] + tdev[1:])

    def block(k, j):
        return ((z - k + nz) % nz) * ny + (y - j + ny) % ny

    def up_part(to):
        return up_ref.at[:, pl.ds(pl.multiple_of(to * units, LANES), units)]

    def dn_part(to):
        return dn_ref.at[pl.ds(pl.multiple_of(to * units, LANES), units), :]

    sent = []

    def start(*args):
        copy = remote(*args)
        copy.start()
        sent.append(copy)

    for k in range(1, nz):
        start(lat_ref.at[mine], lat_out.at[s, mine], lz_s.at[k], lz_r.at[k], zdev[k])
    for j in range(1, ny):
        start(lat_ref.at[mine], lat_out.at[s, mine], ly_s.at[0, j], ly_r.at[0, j], ydev[j])
    for k in range(1, nz):
        to = (z + k) % nz
        start(up_part(to), up_out.at[s], uz_s.at[k], uz_r.at[k], zdev[k])
        start(dn_part(to), dn_out.at[s], dz_s.at[k], dz_r.at[k], zdev[k])
    own = [
        pltpu.make_async_copy(lat_ref, lat_out.at[s], own_sem.at[0]),
        pltpu.make_async_copy(up_part(z), up_out.at[s], own_sem.at[1]),
        pltpu.make_async_copy(dn_part(z), dn_out.at[s], own_sem.at[2]),
    ]
    for copy in own:
        copy.start()

    def to_partner(k, j):
        slot = lat_out.at[block(k, j), mine]
        start(slot, slot, lc_s.at[k, j], lc_r.at[k, j], partner)

    for k in range(1, nz):
        slot = lat_out.at[block(k, 0), mine]
        remote(slot, slot, lz_s.at[k], lz_r.at[k], zdev[k]).wait_recv()
        for j in range(1, ny):
            start(slot, slot, ly_s.at[k, j], ly_r.at[k, j], ydev[j])
        to_partner(k, 0)
    for j in range(1, ny):
        start(up_part(z), up_out.at[s], uy_s.at[0, j], uy_r.at[0, j], ydev[j])
        start(dn_part(z), dn_out.at[s], dy_s.at[0, j], dy_r.at[0, j], ydev[j])
    for k in range(nz):
        for j in range(1, ny):
            slot = lat_out.at[block(k, j), mine]
            remote(slot, slot, ly_s.at[k, j], ly_r.at[k, j], ydev[j]).wait_recv()
            to_partner(k, j)
    for k in range(nz):
        for j in range(ny):
            if k or j:
                slot = lat_out.at[block(k, j), other]
                remote(slot, slot, lc_s.at[k, j], lc_r.at[k, j], partner).wait_recv()
    for copy in own:
        copy.wait()

    def forward(k):
        for out, ss, rs, sy, ry in (
            (up_out, uz_s, uz_r, uy_s, uy_r),
            (dn_out, dz_s, dz_r, dy_s, dy_r),
        ):
            slot = out.at[block(k, 0)]
            remote(slot, slot, ss.at[k], rs.at[k], zdev[k]).wait_recv()
            for j in range(1, ny):
                start(slot, slot, sy.at[k, j], ry.at[k, j], ydev[j])

    rank = wks_ref.shape[0]
    heads = q_ref.shape[0]
    small = wks_ref.shape[1] // (2 * SMALL_DIM)
    row_max[...] = jnp.full_like(row_max, mask_floor)
    row_sum[...] = jnp.zeros_like(row_sum)
    weighted[...] = jnp.zeros_like(weighted)
    ahead = lax.broadcasted_iota(jnp.int32, (rows, rows), 1) - lax.broadcasted_iota(
        jnp.int32, (rows, rows), 0
    )

    def key_step(j, carry):
        latent = lat_out[j, :, :rank]
        turned = lat_out[j, :, rank:]
        kv_small = jnp.dot(latent, wks_ref[...], preferred_element_type=jnp.float32)
        kv_small = kv_small.astype(jnp.bfloat16)
        kv_large = jnp.dot(latent, wkl_ref[...], preferred_element_type=jnp.float32)
        kv_large = kv_large.astype(jnp.bfloat16)
        causal = ahead <= (s - j) * rows
        for h in range(heads):
            if h < small:
                key = kv_small[:, 2 * SMALL_DIM * h : 2 * SMALL_DIM * (h + 1)]
                value = key
                scale = (SMALL_DIM + ROPE_DIM) ** (-0.5)
            else:
                first = 2 * LARGE_DIM * (h - small)
                key = kv_large[:, first : first + LARGE_DIM]
                value = kv_large[:, first + LARGE_DIM : first + 2 * LARGE_DIM]
                scale = (LARGE_DIM + ROPE_DIM) ** (-0.5)
            scores = lax.dot_general(
                q_ref[h],
                jnp.concatenate([key, turned], axis=1),
                (((1,), (1,)), ((), ())),
                preferred_element_type=jnp.float32,
            )
            scores = jnp.where(causal, scores * scale, mask_floor)
            old_max = row_max[h]
            new_max = jnp.maximum(old_max, jnp.max(scores, axis=-1, keepdims=True))
            shrink = jnp.exp(old_max - new_max)
            weights = jnp.exp(scores - new_max)
            row_max[h] = new_max
            row_sum[h] = row_sum[h] * shrink + jnp.sum(weights, axis=-1, keepdims=True)
            weighted[h] = weighted[h] * shrink + jnp.dot(
                weights.astype(jnp.bfloat16), value, preferred_element_type=jnp.float32
            )
        return carry

    middle = (s + 1) // 2
    lax.fori_loop(0, middle, key_step, 0)
    if nz > 1:
        forward(1)
    lax.fori_loop(middle, s + 1, key_step, 0)
    parts = []
    for h in range(heads):
        head_out = (weighted[h] / row_sum[h]).astype(jnp.bfloat16)
        parts.append(head_out[:, SMALL_DIM:] if h < small else head_out)
    mixed_part = jnp.dot(
        jnp.concatenate(parts[:small], axis=1), wos_ref[...], preferred_element_type=jnp.float32
    ) + jnp.dot(
        jnp.concatenate(parts[small:], axis=1), wol_ref[...], preferred_element_type=jnp.float32
    )
    part_ref[...] = mixed_part.astype(jnp.bfloat16).reshape(part_ref.shape)
    rows, width = resid_ref.shape
    for k in range(1, tp):
        start(part_ref.at[(t + k) % tp], rs_in.at[k], a_s.at[k], a_r.at[k], tdev[k])
    for k in range(2, nz - 1):
        forward(k)
    total = resid_ref[...].astype(jnp.float32)
    mixed = part_ref[t].astype(jnp.float32)
    for k in range(1, tp):
        remote(rs_in.at[k], rs_in.at[k], a_s.at[k], a_r.at[k], tdev[k]).wait_recv()
        mixed = mixed + rs_in[k].astype(jnp.float32)
    total = (total + mixed).astype(jnp.bfloat16)
    after[...] = total
    xg[z, c, x] = rms_scale(total, gain_ref[...]).astype(jnp.bfloat16)

    def zi(k):
        return (z - k + nz) % nz

    def xi(j):
        return (x - j + nx) % nx

    def gather_step(k):
        slot = xg.at[zi(k), c, x]
        if k == 0:
            for kk in range(1, nz):
                start(slot, slot, bz_s.at[kk], bz_r.at[kk], zdev[kk])
        else:
            remote(slot, slot, bz_s.at[k], bz_r.at[k], zdev[k]).wait_recv()
        for j in range(1, nx):
            start(slot, slot, bx_s.at[k, j], bx_r.at[k, j], xdev[j])
        start(slot, slot, bc_s.at[k, 0], bc_r.at[k, 0], partner)

    def cross_step(k):
        for j in range(1, nx):
            slot = xg.at[zi(k), c, xi(j)]
            remote(slot, slot, bx_s.at[k, j], bx_r.at[k, j], xdev[j]).wait_recv()
            start(slot, slot, bc_s.at[k, j], bc_r.at[k, j], partner)
        for j in range(nx):
            slot = xg.at[zi(k), 1 - c, xi(j)]
            remote(slot, slot, bc_s.at[k, j], bc_r.at[k, j], partner).wait_recv()

    def compute_step(k):
        tokens = xg[zi(k)].reshape(tp * rows, width)
        projected = jnp.dot(tokens, up_out[...].reshape(width, units), preferred_element_type=jnp.float32)
        hidden = jnp.square(jnp.maximum(projected, 0.0)).astype(jnp.bfloat16)
        cols = dn_out.shape[2]
        for b in range(dn_out.shape[0]):
            block = jnp.dot(hidden, dn_out[b], preferred_element_type=jnp.float32)
            pbuf[k, :, :, :, b * cols : (b + 1) * cols] = block.astype(jnp.bfloat16).reshape(
                CORES, nx, rows, cols
            )
        start(pbuf.at[k, 1 - c], cbuf.at[k], cc_s.at[k], cc_r.at[k], partner)

    def core_sum(k):
        remote(cbuf.at[k], cbuf.at[k], cc_s.at[k], cc_r.at[k], partner).wait_recv()
        pbuf[k, c] = (
            pbuf[k, c].astype(jnp.float32) + cbuf[k].astype(jnp.float32)
        ).astype(jnp.bfloat16)
        for j in range(1, nx):
            start(pbuf.at[k, c, (x + j) % nx], xbuf.at[k, j], cx_s.at[k, j], cx_r.at[k, j], xdev[j])

    def cross_sum(k):
        summed = pbuf[k, c, x].astype(jnp.float32)
        for j in range(1, nx):
            remote(xbuf.at[k, j], xbuf.at[k, j], cx_s.at[k, j], cx_r.at[k, j], xdev[j]).wait_recv()
            summed = summed + xbuf[k, j].astype(jnp.float32)
        zsend[k] = summed.astype(jnp.bfloat16)
        if k:
            start(zsend.at[k], zbuf.at[k], cz_s.at[k], cz_r.at[k], zback[k])

    def weights_here():
        for k in range(nz):
            for j in range(1, ny):
                for out, sy, ry in ((up_out, uy_s, uy_r), (dn_out, dy_s, dy_r)):
                    slot = out.at[block(k, j)]
                    remote(slot, slot, sy.at[k, j], ry.at[k, j], ydev[j]).wait_recv()

    gather_step(0)
    if nz > 2:
        forward(nz - 1)
    for k in range(nz):
        if k + 1 < nz:
            gather_step(k + 1)
        cross_step(k)
        if k == 0:
            weights_here()
        compute_step(k)
        if k >= 2:
            core_sum(k - 1)
        if k >= 3:
            cross_sum(k - 2)
    if nz > 1:
        core_sum(nz - 1)
    core_sum(0)
    for k in range(max(nz - 2, 1), nz):
        cross_sum(k)
    cross_sum(0)
    final = after[...].astype(jnp.float32)
    ffn = zsend[0].astype(jnp.float32)
    for k in range(1, nz):
        remote(zbuf.at[k], zbuf.at[k], cz_s.at[k], cz_r.at[k], zback[k]).wait_recv()
        ffn = ffn + zbuf[k].astype(jnp.float32)
    out_ref[...] = (final + ffn).astype(jnp.bfloat16)
    for copy in sent:
        copy.wait_send()


def layer(ny, nz, nx, latents, q_all, wks, wkl, wos, wol, resid, gain, w_up, w_down):
    tp, sp = nx * CORES, ny * nz
    rows, width = resid.shape
    tok_rows = latents.shape[0]
    heads = q_all.shape[0]
    units = w_up.shape[1] // nz
    dma = pltpu.SemaphoreType.DMA
    vmem = pl.BlockSpec(memory_space=pltpu.VMEM)
    b16 = jnp.bfloat16

    def pair(*shape):
        return [dma(shape), dma(shape)]

    return pl.pallas_call(
        functools.partial(layer_kernel, ny, nz, nx),
        out_shape=jax.ShapeDtypeStruct((rows, width), b16),
        in_specs=[vmem] * 10,
        out_specs=vmem,
        scratch_shapes=[
            pltpu.VMEM((sp,) + latents.shape, b16),
            pltpu.VMEM((sp, w_up.shape[0], units), b16),
            pltpu.VMEM((sp, units, w_down.shape[1]), b16),
            pltpu.VMEM((heads, tok_rows, 1), jnp.float32),
            pltpu.VMEM((heads, tok_rows, 1), jnp.float32),
            pltpu.VMEM((heads, tok_rows, LARGE_DIM), jnp.float32),
            pltpu.VMEM((tp, rows, width), b16),
            pltpu.VMEM((tp, rows, width), b16),
            pltpu.VMEM((rows, width), b16),
            pltpu.VMEM((nz, CORES, nx, rows, width), b16),
            pltpu.VMEM((nz, CORES, nx, rows, width), b16),
            pltpu.VMEM((nz, nx, rows, width), b16),
            pltpu.VMEM((nz, nx, rows, width), b16),
            pltpu.VMEM((nz, rows, width), b16),
            pltpu.VMEM((nz, rows, width), b16),
            dma((3,)),
        ]
        + pair(nz)
        + pair(nz, ny) * 2
        + (pair(nz) + pair(nz, ny)) * 2
        + pair(tp)
        + pair(nz)
        + pair(nz, nx)
        + pair(nz, nx)
        + pair(nz)
        + pair(nz, nx)
        + pair(nz),
        compiler_params=pltpu.CompilerParams(
            collective_id=1, has_side_effects=True, vmem_limit_bytes=63 * 2**20
        ),
        name="layer",
    )(latents, q_all, wks, wkl, wos, wol, resid, gain, w_up, w_down)


def on_device(
    ny,
    nz,
    nx,
    resid,
    q_latent,
    kv_latent,
    rope_key,
    q_gain,
    kv_gain,
    w_q_small,
    w_q_large,
    w_kv_small,
    w_kv_large,
    w_out_small,
    w_out_large,
    ffn_gain,
    w_up,
    w_down,
):
    tok_rows = q_latent.shape[0]
    offset = lax.axis_index("sp") * tok_rows
    positions = offset + jnp.arange(tok_rows, dtype=jnp.int32)
    query_normed = rms_scale(q_latent, q_gain).astype(jnp.bfloat16)
    query_small = queries(query_normed, w_q_small, SMALL_DIM, positions)
    query_large = queries(query_normed, w_q_large, LARGE_DIM, positions)
    key_normed = rms_scale(kv_latent, kv_gain).astype(jnp.bfloat16)
    key_rotated = rotary(rope_key.astype(jnp.float32), positions).astype(jnp.bfloat16)
    rope_pad = ((0, 0), (0, LANES - ROPE_DIM))
    latents = jnp.concatenate([key_normed, jnp.pad(key_rotated, rope_pad)], axis=1)

    def head_rows(query, nope_dim):
        content = jnp.pad(query[..., :nope_dim], ((0, 0), (0, 0), (0, LARGE_DIM - nope_dim)))
        turned = jnp.pad(query[..., nope_dim:], ((0, 0),) + rope_pad)
        return jnp.transpose(jnp.concatenate([content, turned], axis=-1), (1, 0, 2))

    q_all = jnp.concatenate(
        [head_rows(query_small, SMALL_DIM), head_rows(query_large, LARGE_DIM)], axis=0
    )
    return layer(
        ny,
        nz,
        nx,
        latents,
        q_all,
        w_kv_small,
        w_kv_large,
        w_out_small,
        w_out_large,
        resid,
        ffn_gain.reshape(1, -1),
        w_up,
        w_down,
    )


def solution(mesh):
    ny = inner_split(mesh.shape["sp"])
    nz = mesh.shape["sp"] // ny
    nx = mesh.shape["tp"] // CORES
    return jax.shard_map(
        functools.partial(on_device, ny, nz, nx),
        mesh=mesh,
        in_specs=(
            P(("sp", "tp"), None),
            P("sp", None),
            P("sp", None),
            P("sp", None),
            P(),
            P(),
            P(None, "tp"),
            P(None, "tp"),
            P(None, "tp"),
            P(None, "tp"),
            P("tp", None),
            P("tp", None),
            P(),
            P("sp", "tp"),
            P("tp", "sp"),
        ),
        out_specs=P(("sp", "tp"), None),
        check_vma=False,
    )
```

profile of v0, /device:TPU:0, one launch (start us, length us, event | category | flops | bytes accessed | tf_op | source)
XLA Modules:
  0.0 146.4 jit_solution(16965621735946504170)
XLA Ops:
  0.0 0.0 copy-start
  0.0 0.8 convert_element_type.36
  0.8 0.1 multiply_cosine_fusion
  1.0 0.0 copy-start.5
  1.0 1.2 fusion
  2.2 0.0 copy-start.4
  2.2 0.4 fusion.15
  2.6 0.5 copy-done.4
  3.2 0.4 fusion.17
  3.6 0.1 copy.31
  3.7 0.1 copy.34
  3.9 0.1 copy.33
  4.0 0.1 copy.35
  4.2 0.1 fusion.14
  4.2 0.0 copy-start.1
  4.2 0.8 pad_maximum_fusion.q_ref
  5.1 0.1 copy.29
  5.2 0.1 fusion.4
  5.3 0.0 copy-start.3
  5.4 0.7 copy-done.3
  6.0 0.1 fusion.6
  6.2 0.8 fusion.10.lat_ref
  6.9 137.9 %layer.1 = bf16[64,2048]{1,0:T(8,128)(2,1)} custom-call(bf16[256,640]{1,0:T(8,128)(2,1)} %fusion.10.lat_ref, bf16[4,256,256]{2,1,0:T(8,128)(2,1)} %pad_maximum_fusion.q_ref, bf16[512,256]{1,0:T(8,128)(2,1)} %wks_ref.1, bf16[512,512]{1,0:T(8,128)(2,1)} %wkl_ref.1, bf16[128,2048]{1,0:T(8,128)(2,1)} %wos_ref.1, bf16[256,2048]{1,0:T(8,128)(2,1)} %wol_ref.1, ...), custom_call_target="tpu_custom_call" | custom-call | tf_op jit(solution)/shard_map/layer/pallas_call | solution.py:368
  144.8 1.7 %copy.37 = bf16[64,2048]{1,0:T(8,128)(2,1)} copy(bf16[64,2048]{1,0:T(8,128)(2,1)} %layer.1) | data formatting | bytes 524288
  (15 shorter events, 0.1 us)
Async XLA Ops:
  0.0 2.2 %copy-start = (bf16[768,320]{0,1:T(8,128)(2,1)S(1)}, bf16[768,320]{0,1:T(8,128)(2,1)}, u32[]{:S(2)}) copy-start(bf16[768,320]{0,1:T(8,128)(2,1)} %param.22) | copy-start | bytes 1474564
  0.0 2.2 %copy-start.2 = (bf16[256,768]{1,0:T(8,128)(2,1)S(1)}, bf16[256,768]{1,0:T(8,128)(2,1)}, u32[]{:S(2)}) copy-start(bf16[256,768]{1,0:T(8,128)(2,1)} %param.16) | copy-start | bytes 1179652
  1.0 1.2 copy-start.5
  2.2 1.0 copy-start.4
  4.2 1.0 copy-start.1
  5.3 0.7 copy-start.3
where the time goes:
time: 147 us; the launch traced here: 146 us
  Pallas kernels  138 us (94%)
  other arithmetic  4.12 us (3%)
  local copies, waits for them, and re-layouts  3.54 us (2%)
    pallas_call x1, Pallas kernels, layer(): pl.pallas_call(functools.partial(layer_kernel, ny, nz, nx), out_shape=jax...  138 us
    unnamed x15, local copies, waits for them, and re-layouts  3.14 us

commit v1 on v0

v1 whole, which is shorter than its diff:
```python
import functools

import jax
import jax.numpy as jnp
from jax import lax
from jax.experimental import pallas as pl
from jax.experimental.pallas import tpu as pltpu
from jax.sharding import PartitionSpec as P

SMALL_DIM = 64
LARGE_DIM = 128
ROPE_DIM = 32
HALF_ROPE = ROPE_DIM // 2

epsilon = 1e-06
theta_base = 10000.0
LOG2E = 1.4426950408889634

MESH = pl.DeviceIdType.MESH
CORES = 2
LANES = 128
HALVES = 2


def rms_scale(inputs, gain_vec):
    values = inputs.astype(jnp.float32)
    return (
        values * lax.rsqrt(jnp.mean(values * values, axis=-1, keepdims=True) + epsilon) * gain_vec
    )


def rotary_tables(positions):
    lane = jnp.arange(LANES, dtype=jnp.int32)
    exponent = (2 * (lane % HALF_ROPE)).astype(jnp.float32) / ROPE_DIM
    angles = positions.astype(jnp.float32)[:, None] * (theta_base ** (-exponent))[None, :]
    inside = (lane < ROPE_DIM)[None, :]
    sign = jnp.where(lane < HALF_ROPE, -1.0, 1.0)[None, :]
    return jnp.where(inside, jnp.cos(angles), 0.0), jnp.where(inside, sign * jnp.sin(angles), 0.0)


def inner_split(count):
    best = 1
    for size in range(1, count + 1):
        if size * size <= count and count % size == 0:
            best = size
    return best


def near_first(count):
    return sorted(range(1, count), key=lambda k: (min(k, count - k), k))


def remote(src, dst, send_sem, recv_sem, device):
    return pltpu.make_async_remote_copy(
        src_ref=src,
        dst_ref=dst,
        send_sem=send_sem,
        recv_sem=recv_sem,
        device_id=device,
        device_id_type=MESH,
    )


def place(ny, nz, nx):
    s, t = lax.axis_index("sp"), lax.axis_index("tp")
    z, y = s // ny, s % ny
    x, c = t // CORES, t % CORES

    def at(zz, yy, xx, cc):
        return (zz * ny + yy, xx * CORES + cc)

    return z, y, x, c, at


def layer_kernel(
    ny, nz, nx,
    q_lat, kv_lat, rope_key, cos_ref, sin_ref, q_gain, kv_gain, gain_ref, resid_ref,
    wqs_hbm, wql_hbm, wks_hbm, wkl_hbm, wos_hbm, wol_hbm, up_ref, dn_ref, out_ref,
    lat_out, up_out, dn_out, wqs, wql, wks, wkl, wos, wol, spread_ref, q_all,
    row_max, row_sum, weighted, part_ref, rs_c, rs_x, after, xg, hid,
    pbuf, cbuf, xbuf, zsend, zbuf, own_sem,
    lz_s, lz_r, ly_s, ly_r, lx_s, lx_r, lc_s, lc_r,
    uz_s, uz_r, uy_s, uy_r, dz_s, dz_r, dy_s, dy_r,
    ac_s, ac_r, ax_s, ax_r, bz_s, bz_r, bx_s, bx_r, bc_s, bc_r,
    cc_s, cc_r, cx_s, cx_r, cz_s, cz_r,
):
    z, y, x, c, at = place(ny, nz, nx)
    s = z * ny + y
    tp = nx * CORES
    t = x * CORES + c
    tok_rows = lat_out.shape[1]
    part = tok_rows // tp
    rank = kv_lat.shape[1]
    units = up_out.shape[2]
    rows, width = resid_ref.shape
    heads = q_all.shape[0]
    small = wks.shape[1] // (2 * SMALL_DIM)
    partner = at(z, y, x, 1 - c)
    zdev = [at((z + k) % nz, y, x, c) for k in range(nz)]
    zback = [at((z - k + nz) % nz, y, x, c) for k in range(nz)]
    ydev = [at(z, (y + j) % ny, x, c) for j in range(ny)]
    xdev = [at(z, y, (x + i) % nx, c) for i in range(nx)]
    zorder = near_first(nz)

    barrier = pltpu.get_barrier_semaphore()
    friends = zdev[1:] + ydev[1:] + xdev[1:] + [partner]
    for device in friends:
        pl.semaphore_signal(barrier, inc=1, device_id=device, device_id_type=MESH)

    def up_part(to):
        return up_ref.at[:, pl.ds(pl.multiple_of(to * units, LANES), units)]

    def dn_part(to):
        return dn_ref.at[pl.ds(pl.multiple_of(to * units, LANES), units), :]

    local = [
        pltpu.make_async_copy(src, dst, own_sem.at[i])
        for i, (src, dst) in enumerate(
            (
                (wqs_hbm, wqs),
                (wql_hbm, wql),
                (wks_hbm, wks),
                (wkl_hbm, wkl),
                (wos_hbm, wos),
                (wol_hbm, wol),
                (up_part(z), up_out.at[s]),
                (dn_part(z), dn_out.at[s]),
            )
        )
    ]
    for copy in local:
        copy.start()

    sent = []
    guard = [None]

    def start(make):
        sent.append((guard[-1], make))
        remote(*make()).start()

    def under(condition, body):
        guard.append(condition)
        pl.when(condition)(body)
        guard.pop()

    def arrive(make):
        remote(*make()).wait_recv()

    def zi(k):
        return (z - k + nz) % nz

    def block(k, j):
        return zi(k) * ny + (y - j + ny) % ny

    lane = lax.broadcasted_iota(jnp.int32, (tok_rows, LANES), 1)

    def turn(values):
        swapped = jnp.where(
            lane < HALF_ROPE,
            pltpu.roll(values, LANES - HALF_ROPE, 1),
            pltpu.roll(values, HALF_ROPE, 1),
        )
        turned = values * cos_ref[...] + swapped * sin_ref[...]
        return jnp.where(lane < ROPE_DIM, turned, 0.0)

    spread_ref[...] = jnp.zeros_like(spread_ref)
    spread_ref[:, :ROPE_DIM] = rope_key[...].astype(jnp.float32)
    lat_out[s, :, :rank] = rms_scale(kv_lat[...], kv_gain[...]).astype(jnp.bfloat16)
    lat_out[s, :, rank:] = turn(spread_ref[:, :LANES]).astype(jnp.bfloat16)

    with jax.named_scope("greet"):
        pl.semaphore_wait(barrier, len(friends))

    def share(b, p):
        return lat_out.at[b, pl.ds(pl.multiple_of(p * part, part), part)]

    def at_part(i, cc):
        return ((x - i + nx) % nx) * CORES + cc

    def lz(k, b):
        return lambda: (share(b(), t), share(b(), t), lz_s.at[k], lz_r.at[k], zdev[k])

    def ly(k, j, b):
        return lambda: (share(b(), t), share(b(), t), ly_s.at[k, j], ly_r.at[k, j], ydev[j])

    def lx(k, j, i, p):
        return lambda: (
            share(block(k, j), p()), share(block(k, j), p()),
            lx_s.at[k, j, i], lx_r.at[k, j, i], xdev[i],
        )

    def lc(k, j, i, cc):
        return lambda: (
            share(block(k, j), at_part(i, cc)), share(block(k, j), at_part(i, cc)),
            lc_s.at[k, j, i], lc_r.at[k, j, i], partner,
        )

    def lat_spread(k, j):
        for i in range(1, nx):
            start(lx(k, j, i, lambda: t))
        start(lc(k, j, 0, c))

    for k in zorder:
        under(z + k < nz, lambda k=k: start(lz(k, lambda: s)))
    for j in range(1, ny):
        under(y + j < ny, lambda j=j: start(ly(0, j, lambda: s)))

    def z_up(k):
        return lambda: (up_part((z + k) % nz), up_out.at[s], uz_s.at[k], uz_r.at[k], zdev[k])

    def z_dn(k):
        return lambda: (dn_part((z + k) % nz), dn_out.at[s], dz_s.at[k], dz_r.at[k], zdev[k])

    for k in zorder:
        start(z_up(k))
    for k in zorder:
        start(z_dn(k))
    for j in range(1, ny):
        start(lambda j=j: (up_part(z), up_out.at[s], uy_s.at[0, j], uy_r.at[0, j], ydev[j]))

    def up_forward(k):
        slot = lambda: up_out.at[block(k, 0)]
        arrive(lambda: (slot(), slot(), uz_s.at[k], uz_r.at[k], zdev[k]))
        for j in range(1, ny):
            start(lambda j=j: (slot(), slot(), uy_s.at[k, j], uy_r.at[k, j], ydev[j]))

    def dn_forward(k):
        slot = lambda: dn_out.at[block(k, 0)]
        arrive(lambda: (slot(), slot(), dz_s.at[k], dz_r.at[k], zdev[k]))
        for j in range(1, ny):
            start(lambda j=j: (slot(), slot(), dy_s.at[k, j], dy_r.at[k, j], ydev[j]))

    with jax.named_scope("queries"):
        query_normed = rms_scale(q_lat[...], q_gain[...]).astype(jnp.bfloat16)
        head = 0
        for w_ref, copies, nope in ((wqs, local[0], SMALL_DIM), (wql, local[1], LARGE_DIM)):
            copies.wait()
            cols = w_ref.shape[1]
            spread_ref[:, :cols] = jnp.dot(
                query_normed, w_ref[...], preferred_element_type=jnp.float32
            )

            def take(first, size):
                b, off = first // LANES, first % LANES
                got = spread_ref[:, b * LANES : (b + 1) * LANES]
                if off:
                    got = pltpu.roll(got, LANES - off, 1)
                if off + size > LANES:
                    more = spread_ref[:, (b + 1) * LANES : (b + 2) * LANES]
                    got = jnp.where(lane < LANES - off, got, pltpu.roll(more, LANES - off, 1))
                return got

            for h in range(cols // (nope + ROPE_DIM)):
                first = h * (nope + ROPE_DIM)
                content = take(first, nope)
                if nope < LANES:
                    content = jnp.where(lane < nope, content, 0.0)
                q_all[head, :, :LANES] = content.astype(jnp.bfloat16)
                q_all[head, :, LANES:] = turn(take(first + nope, ROPE_DIM)).astype(jnp.bfloat16)
                head += 1
    local[2].wait()
    local[3].wait()

    def attend(latents, causal, first):
        latent = latents[:, :rank]
        turned = latents[:, rank:]
        kv_small = jnp.dot(latent, wks[...], preferred_element_type=jnp.float32)
        kv_small = kv_small.astype(jnp.bfloat16)
        kv_large = jnp.dot(latent, wkl[...], preferred_element_type=jnp.float32)
        kv_large = kv_large.astype(jnp.bfloat16)
        for h in range(heads):
            if h < small:
                key = kv_small[:, 2 * SMALL_DIM * h : 2 * SMALL_DIM * (h + 1)]
                value = key
                scale = (SMALL_DIM + ROPE_DIM) ** (-0.5)
            else:
                begin = 2 * LARGE_DIM * (h - small)
                key = kv_large[:, begin : begin + LARGE_DIM]
                value = kv_large[:, begin + LARGE_DIM : begin + 2 * LARGE_DIM]
                scale = (LARGE_DIM + ROPE_DIM) ** (-0.5)
            scores = lax.dot_general(
                q_all[h],
                jnp.concatenate([key, turned], axis=1),
                (((1,), (1,)), ((), ())),
                preferred_element_type=jnp.float32,
            )
            scores = scores * (scale * LOG2E)
            if causal is not None:
                scores = jnp.where(causal, scores, -1e30)
            top = jnp.max(scores, axis=-1, keepdims=True)
            if first:
                weights = jnp.exp2(scores - top)
                row_max[h] = top
                row_sum[h] = jnp.sum(weights, axis=-1, keepdims=True)
                weighted[h] = jnp.dot(
                    weights.astype(jnp.bfloat16), value, preferred_element_type=jnp.float32
                )
                continue
            old_max = row_max[h]
            new_max = jnp.maximum(old_max, top)
            shrink = jnp.exp2(old_max - new_max)
            weights = jnp.exp2(scores - new_max)
            row_max[h] = new_max
            row_sum[h] = row_sum[h] * shrink + jnp.sum(weights, axis=-1, keepdims=True)
            weighted[h] = weighted[h] * shrink + jnp.dot(
                weights.astype(jnp.bfloat16), value, preferred_element_type=jnp.float32
            )

    def lat_from_z(k):
        slot = lambda: block(k, 0)
        arrive(lz(k, slot))
        for j in range(1, ny):
            start(ly(k, j, slot))
        lat_spread(k, 0)

    def lat_from_y(k, j):
        arrive(ly(k, j, lambda: block(k, j)))
        lat_spread(k, j)

    def lat_from_x(k, j):
        for i in range(1, nx):
            arrive(lx(k, j, i, lambda i=i: at_part(i, c)))
            start(lc(k, j, i, c))

    def lat_here(k, j):
        for i in range(nx):
            arrive(lc(k, j, i, 1 - c))

    with jax.named_scope("own"):
        ahead = lax.broadcasted_iota(jnp.int32, (tok_rows, tok_rows), 1) <= (
            lax.broadcasted_iota(jnp.int32, (tok_rows, tok_rows), 0)
        )
        attend(lat_out[s], ahead, True)
    with jax.named_scope("lat_z"):
        for k in zorder:
            under(z >= k, lambda k=k: lat_from_z(k))
        for j in range(1, ny):
            under(y >= j, lambda j=j: lat_from_y(0, j))
    for j in range(1, ny):
        start(lambda j=j: (dn_part(z), dn_out.at[s], dy_s.at[0, j], dy_r.at[0, j], ydev[j]))
    with jax.named_scope("lat_x0"):
        for j in range(1, ny):
            under(y >= j, lambda j=j: lat_from_x(0, j))
        for k in zorder:
            under(z >= k, lambda k=k: lat_from_x(k, 0))
        for j in range(1, ny):
            under(y >= j, lambda j=j: lat_here(0, j))
    with jax.named_scope("near"):
        def near(j, carry):
            attend(lat_out[z * ny + j], None, False)
            return carry

        lax.fori_loop(0, y, near, 0)
    with jax.named_scope("lat_y"):
        for k in zorder:
            for j in range(1, ny):
                under(z >= k, lambda k=k, j=j: lat_from_y(k, j))
        for k in zorder:
            for j in range(1, ny):
                under(z >= k, lambda k=k, j=j: lat_from_x(k, j))
    with jax.named_scope("up_fwd"):
        for k in zorder[:2]:
            up_forward(k)
    with jax.named_scope("lat_all"):
        for k in zorder:
            for j in range(ny):
                under(z >= k, lambda k=k, j=j: lat_here(k, j))
    with jax.named_scope("far"):
        def far(zz, carry):
            latents = lat_out[pl.ds(zz * ny, ny)].reshape(ny * tok_rows, lat_out.shape[2])
            attend(latents, None, False)
            return carry

        lax.fori_loop(0, z, far, 0)
    local[4].wait()
    local[5].wait()
    with jax.named_scope("outproj"):
        parts = []
        for h in range(heads):
            head_out = (weighted[h] / row_sum[h]).astype(jnp.bfloat16)
            parts.append(head_out[:, SMALL_DIM:] if h < small else head_out)
        from_small = jnp.concatenate(parts[:small], axis=1)
        from_large = jnp.concatenate(parts[small:], axis=1)
        cut = width // HALVES

        def ac(i):
            return lambda: (part_ref.at[i, 1 - c], rs_c.at[i], ac_s.at[i], ac_r.at[i], partner)

        def ax(i, j):
            return lambda: (
                part_ref.at[i, c, (x + j) % nx], rs_x.at[i, j], ax_s.at[i, j], ax_r.at[i, j], xdev[j]
            )

        for i in range(HALVES):
            mixed = jnp.dot(
                from_small, wos[:, i * cut : (i + 1) * cut], preferred_element_type=jnp.float32
            ) + jnp.dot(
                from_large, wol[:, i * cut : (i + 1) * cut], preferred_element_type=jnp.float32
            )
            mixed = mixed.astype(jnp.bfloat16)
            for xx in range(nx):
                for cc in range(CORES):
                    first = (xx * CORES + cc) * rows
                    part_ref[i, cc, xx] = mixed[first : first + rows]
            start(ac(i))
    with jax.named_scope("rs_core"):
        for i in range(HALVES):
            arrive(ac(i))
            part_ref[i, c] = (
                part_ref[i, c].astype(jnp.float32) + rs_c[i].astype(jnp.float32)
            ).astype(jnp.bfloat16)
            for j in range(1, nx):
                start(ax(i, j))
    with jax.named_scope("fwd2"):
        for k in zorder[2:]:
            up_forward(k)
        for k in zorder[:2]:
            dn_forward(k)
    with jax.named_scope("rs_x"):
        for i in range(HALVES):
            mixed = part_ref[i, c, x].astype(jnp.float32)
            for j in range(1, nx):
                arrive(ax(i, j))
                mixed = mixed + rs_x[i, j].astype(jnp.float32)
            piece = resid_ref[:, i * cut : (i + 1) * cut].astype(jnp.float32) + mixed
            after[:, i * cut : (i + 1) * cut] = piece.astype(jnp.bfloat16)
        xg[z, c, x] = rms_scale(after[...], gain_ref[...]).astype(jnp.bfloat16)

    def bz(k):
        slot = lambda: xg.at[z, c, x]
        return lambda: (slot(), slot(), bz_s.at[k], bz_r.at[z], zdev[k])

    def spread(a):
        slot = lambda: xg.at[a, c, x]
        for i in range(1, nx):
            start(lambda i=i: (slot(), slot(), bx_s.at[a, i], bx_r.at[a, i], xdev[i]))
        start(lambda: (slot(), slot(), bc_s.at[a, 0], bc_r.at[a, 0], partner))

    for k in zorder:
        start(bz(k))
    spread(z)
    with jax.named_scope("fwd3"):
        for k in zorder[2:]:
            dn_forward(k)
    with jax.named_scope("g_z"):
        for a in range(nz):
            def from_z(a=a):
                slot = lambda: xg.at[a, c, x]
                arrive(lambda: (slot(), slot(), bz_s.at[0], bz_r.at[a], partner))
                for i in range(1, nx):
                    start(lambda i=i: (slot(), slot(), bx_s.at[a, i], bx_r.at[a, i], xdev[i]))
                start(lambda: (slot(), slot(), bc_s.at[a, 0], bc_r.at[a, 0], partner))

            under(z != a, from_z)

    def xi(i):
        return (x - i + nx) % nx

    def from_x(a):
        for i in range(1, nx):
            slot = lambda i=i: xg.at[a, c, xi(i)]
            arrive(lambda: (slot(), slot(), bx_s.at[a, i], bx_r.at[a, i], xdev[i]))
            start(lambda i=i, slot=slot: (slot(), slot(), bc_s.at[a, i], bc_r.at[a, i], partner))

    def rows_here(a):
        for i in range(nx):
            slot = lambda i=i: xg.at[a, 1 - c, xi(i)]
            arrive(lambda: (slot(), slot(), bc_s.at[a, i], bc_r.at[a, i], partner))

    def weights_here(out, sy, ry):
        for k in range(nz):
            for j in range(1, ny):
                slot = lambda: out.at[block(k, j)]
                arrive(lambda: (slot(), slot(), sy.at[k, j], ry.at[k, j], ydev[j]))

    def up_step(a):
        rows_here(a)
        tokens = xg[a].reshape(tp * rows, width)
        projected = jnp.dot(
            tokens, up_out[...].reshape(width, units), preferred_element_type=jnp.float32
        )
        hid[a] = jnp.square(jnp.maximum(projected, 0.0)).astype(jnp.bfloat16)

    def down_step(k):
        hidden = hid[zi(k)]
        cols = dn_out.shape[2]
        for b in range(dn_out.shape[0]):
            out = jnp.dot(hidden, dn_out[b], preferred_element_type=jnp.float32)
            pbuf[k, :, :, :, b * cols : (b + 1) * cols] = out.astype(jnp.bfloat16).reshape(
                CORES, nx, rows, cols
            )
        start(lambda: (pbuf.at[k, 1 - c], cbuf.at[k], cc_s.at[k], cc_r.at[k], partner))

    def core_sum(k):
        arrive(lambda: (cbuf.at[k], cbuf.at[k], cc_s.at[k], cc_r.at[k], partner))
        pbuf[k, c] = (
            pbuf[k, c].astype(jnp.float32) + cbuf[k].astype(jnp.float32)
        ).astype(jnp.bfloat16)
        for j in range(1, nx):
            start(
                lambda j=j: (
                    pbuf.at[k, c, (x + j) % nx], xbuf.at[k, j], cx_s.at[k, j], cx_r.at[k, j], xdev[j]
                )
            )

    def cross_sum(k):
        summed = pbuf[k, c, x].astype(jnp.float32)
        for j in range(1, nx):
            arrive(lambda: (xbuf.at[k, j], xbuf.at[k, j], cx_s.at[k, j], cx_r.at[k, j], xdev[j]))
            summed = summed + xbuf[k, j].astype(jnp.float32)
        zsend[k] = summed.astype(jnp.bfloat16)
        if k:
            start(lambda: (zsend.at[k], zbuf.at[k], cz_s.at[k], cz_r.at[k], zback[k]))

    with jax.named_scope("g_x"):
        from_x(0)
    local[6].wait()
    with jax.named_scope("w_up"):
        weights_here(up_out, uy_s, uy_r)
    for a in range(nz):
        if a + 1 < nz:
            with jax.named_scope("g_x"):
                from_x(a + 1)
        with jax.named_scope("up"):
            up_step(a)
    local[7].wait()
    with jax.named_scope("w_dn"):
        weights_here(dn_out, dy_s, dy_r)
    order = zorder[::-1] + [0]
    with jax.named_scope("down"):
        for i, k in enumerate(order):
            down_step(k)
            if i:
                core_sum(order[i - 1])
        core_sum(order[-1])
    for k in order:
        with jax.named_scope("cross"):
            cross_sum(k)
    with jax.named_scope("final"):
        final = after[...].astype(jnp.float32)
        ffn = zsend[0].astype(jnp.float32)
        for k in order[:-1]:
            arrive(lambda: (zbuf.at[k], zbuf.at[k], cz_s.at[k], cz_r.at[k], zback[k]))
            ffn = ffn + zbuf[k].astype(jnp.float32)
        out_ref[...] = (final + ffn).astype(jnp.bfloat16)

    def finish(make):
        remote(*make()).wait_send()

    with jax.named_scope("wait_send"):
        for condition, make in sent:
            if condition is None:
                finish(make)
            else:
                pl.when(condition)(functools.partial(finish, make))


def layer(
    ny, nz, nx, q_lat, kv_lat, rope_key, cos, sin, q_gain, kv_gain, gain, resid,
    wqs, wql, wks, wkl, wos, wol, w_up, w_down,
):
    tp, sp = nx * CORES, ny * nz
    rows, width = resid.shape
    tok_rows, rank = kv_lat.shape
    small = wks.shape[1] // (2 * SMALL_DIM)
    large = wkl.shape[1] // (2 * LARGE_DIM)
    heads = small + large
    units = w_up.shape[1] // nz
    query_cols = -(-max(wqs.shape[1], wql.shape[1]) // LANES) * LANES
    dma = pltpu.SemaphoreType.DMA
    vmem = pl.BlockSpec(memory_space=pltpu.VMEM)
    anywhere = pl.BlockSpec(memory_space=pl.ANY)
    b16, f32 = jnp.bfloat16, jnp.float32

    def pair(*shape):
        return [dma(shape), dma(shape)]

    def like(array):
        return pltpu.VMEM(array.shape, array.dtype)

    return pl.pallas_call(
        functools.partial(layer_kernel, ny, nz, nx),
        out_shape=jax.ShapeDtypeStruct((rows, width), b16),
        in_specs=[vmem] * 9 + [anywhere] * 8,
        out_specs=vmem,
        scratch_shapes=[
            pltpu.VMEM((sp, tok_rows, rank + LANES), b16),
            pltpu.VMEM((sp, w_up.shape[0], units), b16),
            pltpu.VMEM((sp, units, w_down.shape[1]), b16),
            like(wqs),
            like(wql),
            like(wks),
            like(wkl),
            like(wos),
            like(wol),
            pltpu.VMEM((tok_rows, query_cols), f32),
            pltpu.VMEM((heads, tok_rows, 2 * LANES), b16),
            pltpu.VMEM((heads, tok_rows, 1), f32),
            pltpu.VMEM((heads, tok_rows, 1), f32),
            pltpu.VMEM((heads, tok_rows, LARGE_DIM), f32),
            pltpu.VMEM((HALVES, CORES, nx, rows, width // HALVES), b16),
            pltpu.VMEM((HALVES, nx, rows, width // HALVES), b16),
            pltpu.VMEM((HALVES, nx, rows, width // HALVES), b16),
            pltpu.VMEM((rows, width), b16),
            pltpu.VMEM((nz, CORES, nx, rows, width), b16),
            pltpu.VMEM((nz, tp * rows, units), b16),
            pltpu.VMEM((nz, CORES, nx, rows, width), b16),
            pltpu.VMEM((nz, nx, rows, width), b16),
            pltpu.VMEM((nz, nx, rows, width), b16),
            pltpu.VMEM((nz, rows, width), b16),
            pltpu.VMEM((nz, rows, width), b16),
            dma((8,)),
        ]
        + pair(nz)
        + pair(nz, ny)
        + pair(nz, ny, nx) * 2
        + (pair(nz) + pair(nz, ny)) * 2
        + pair(HALVES)
        + pair(HALVES, nx)
        + pair(nz)
        + pair(nz, nx) * 2
        + pair(nz)
        + pair(nz, nx)
        + pair(nz),
        compiler_params=pltpu.CompilerParams(
            collective_id=1, has_side_effects=True, vmem_limit_bytes=63 * 2**20
        ),
        name="layer",
    )(
        q_lat, kv_lat, rope_key, cos, sin, q_gain, kv_gain, gain, resid,
        wqs, wql, wks, wkl, wos, wol, w_up, w_down,
    )


def on_device(
    ny,
    nz,
    nx,
    resid,
    q_latent,
    kv_latent,
    rope_key,
    q_gain,
    kv_gain,
    w_q_small,
    w_q_large,
    w_kv_small,
    w_kv_large,
    w_out_small,
    w_out_large,
    ffn_gain,
    w_up,
    w_down,
):
    tok_rows = q_latent.shape[0]
    offset = lax.axis_index("sp") * tok_rows
    cos, sin = rotary_tables(offset + jnp.arange(tok_rows, dtype=jnp.int32))
    return layer(
        ny,
        nz,
        nx,
        q_latent,
        kv_latent,
        rope_key,
        cos,
        sin,
        q_gain.reshape(1, -1),
        kv_gain.reshape(1, -1),
        ffn_gain.reshape(1, -1),
        resid,
        w_q_small,
        w_q_large,
        w_kv_small,
        w_kv_large,
        w_out_small,
        w_out_large,
        w_up,
        w_down,
    )


def solution(mesh):
    ny = inner_split(mesh.shape["sp"])
    nz = mesh.shape["sp"] // ny
    nx = mesh.shape["tp"] // CORES
    return jax.shard_map(
        functools.partial(on_device, ny, nz, nx),
        mesh=mesh,
        in_specs=(
            P(("sp", "tp"), None),
            P("sp", None),
            P("sp", None),
            P("sp", None),
            P(),
            P(),
            P(None, "tp"),
            P(None, "tp"),
            P(None, "tp"),
            P(None, "tp"),
            P("tp", None),
            P("tp", None),
            P(),
            P("sp", "tp"),
            P("tp", "sp"),
        ),
        out_specs=P(("sp", "tp"), None),
        check_vma=False,
    )
```

time: 147 us -> 134 us (0.912)
  the two profiles are of different devices: /device:TPU:0 before, /device:TPU:15 now
where the time goes in v1:
time: 134 us
  Pallas kernels  126 us (94%)
  local copies, waits for them, and re-layouts  6.41 us (5%)
    pallas_call x1, Pallas kernels, layer(): pl.pallas_call(functools.partial(layer_kernel, ny, nz, nx), out_shape=jax...  126 us
    unnamed x8, local copies, waits for them, and re-layouts  5.1 us

profile of v1, /device:TPU:15, one launch (start us, length us, event | category | flops | bytes accessed | tf_op | source)
XLA Modules:
  0.0 134.0 jit_solution(3792994507928125796)
XLA Ops:
  0.0 0.0 copy-start.1
  0.0 1.3 reshape.37.q_gain
  1.3 1.4 %copy.16.rope_key = bf16[256,32]{1,0:T(8,128)(2,1)} copy(bf16[256,32]{0,1:T(8,128)(2,1)} %param.18) | data formatting | bytes 32768 | tf_op args[3]
  2.8 0.0 copy-start
  2.8 1.2 fusion.2
  4.0 0.0 copy-done.1
  4.0 0.9 copy.17.wqs_hbm
  5.0 0.0 copy-done
  5.0 1.1 copy.18.wql_hbm
  6.0 126.3 %layer.1 = bf16[64,2048]{1,0:T(8,128)(2,1)} custom-call(bf16[256,768]{1,0:T(8,128)(2,1)} %q_lat.1, bf16[256,512]{1,0:T(8,128)(2,1)} %kv_lat.1, bf16[256,32]{1,0:T(8,128)(2,1)} %copy.16.rope_key, f32[256,128]{1,0:T(8,128)} %get-tuple-element.6.cos_ref, f32[256,128]{1,0:T(8,128)} %get-tuple-element.5.sin_ref, f32[1,768]{1,0:T(1,128)} %reshape.37.q_gain, ...), custom_call_target="tpu_custom_call" | custom-call | tf_op jit(solution)/shard_map/layer/pallas_call | solution.py:581
  132.3 1.7 %copy.20 = bf16[64,2048]{1,0:T(8,128)(2,1)} copy(bf16[64,2048]{1,0:T(8,128)(2,1)} %layer.1) | data formatting | bytes 524288
  (3 shorter events, 0.0 us)
Async XLA Ops:
  0.0 4.0 %copy-start.1 = (bf16[768,192]{0,1:T(8,128)(2,1)S(1)}, bf16[768,192]{0,1:T(8,128)(2,1)}, u32[]{:S(2)}) copy-start(bf16[768,192]{0,1:T(8,128)(2,1)} %param.21) | copy-start | bytes 884740
  2.8 2.2 %copy-start = (bf16[768,320]{0,1:T(8,128)(2,1)S(1)}, bf16[768,320]{0,1:T(8,128)(2,1)}, u32[]{:S(2)}) copy-start(bf16[768,320]{0,1:T(8,128)(2,1)} %param.22) | copy-start | bytes 1474564

commit v2 on v1

--- a/solution.py
+++ b/solution.py
@@ -30,12 +30,9 @@
 
 
 def rotary_tables(positions):
-    lane = jnp.arange(LANES, dtype=jnp.int32)
-    exponent = (2 * (lane % HALF_ROPE)).astype(jnp.float32) / ROPE_DIM
-    angles = positions.astype(jnp.float32)[:, None] * (theta_base ** (-exponent))[None, :]
-    inside = (lane < ROPE_DIM)[None, :]
-    sign = jnp.where(lane < HALF_ROPE, -1.0, 1.0)[None, :]
-    return jnp.where(inside, jnp.cos(angles), 0.0), jnp.where(inside, sign * jnp.sin(angles), 0.0)
+    exponent = jnp.arange(0, ROPE_DIM, 2, dtype=jnp.float32) / ROPE_DIM
+    angles = (theta_base ** (-exponent))[:, None] * positions.astype(jnp.float32)[None, :]
+    return jnp.cos(angles), jnp.sin(angles)
 
 
 def inner_split(count):
@@ -46,8 +43,15 @@
     return best
 
 
-def near_first(count):
-    return sorted(range(1, count), key=lambda k: (min(k, count - k), k))
+def outward(count, z, i):
+    orders = [
+        sorted(range(count), key=lambda a: (abs(a - zz), a if 2 * zz < count else -a))
+        for zz in range(count)
+    ]
+    got = orders[0][i]
+    for zz in range(1, count):
+        got = got + jnp.minimum(jnp.maximum(z - (zz - 1), 0), 1) * (orders[zz][i] - orders[zz - 1][i])
+    return got
 
 
 def remote(src, dst, send_sem, recv_sem, device):
@@ -74,14 +78,14 @@
 
 def layer_kernel(
     ny, nz, nx,
-    q_lat, kv_lat, rope_key, cos_ref, sin_ref, q_gain, kv_gain, gain_ref, resid_ref,
+    q_lat, kv_lat, rope_t, cos_t, sin_t, q_gain, kv_gain, gain_ref, resid_ref,
     wqs_hbm, wql_hbm, wks_hbm, wkl_hbm, wos_hbm, wol_hbm, up_ref, dn_ref, out_ref,
-    lat_out, up_out, dn_out, wqs, wql, wks, wkl, wos, wol, spread_ref, q_all,
+    lat_out, up_out, dn_out, wqs, wql, wks, wkl, wos, wol, stood, spread_ref, q_all,
     row_max, row_sum, weighted, part_ref, rs_c, rs_x, after, xg, hid,
-    pbuf, cbuf, xbuf, zsend, zbuf, own_sem,
+    pbuf, cbuf, xbuf, zsend, zbuf, own_sem, go_sem,
     lz_s, lz_r, ly_s, ly_r, lx_s, lx_r, lc_s, lc_r,
     uz_s, uz_r, uy_s, uy_r, dz_s, dz_r, dy_s, dy_r,
-    ac_s, ac_r, ax_s, ax_r, bz_s, bz_r, bx_s, bx_r, bc_s, bc_r,
+    ac_s, ac_r, ax_s, ax_r, bz_s, bz_r, bo_s, bx_s, bx_r, bc_s, bc_r,
     cc_s, cc_r, cx_s, cx_r, cz_s, cz_r,
 ):
     z, y, x, c, at = place(ny, nz, nx)
@@ -97,10 +101,11 @@
     small = wks.shape[1] // (2 * SMALL_DIM)
     partner = at(z, y, x, 1 - c)
     zdev = [at((z + k) % nz, y, x, c) for k in range(nz)]
-    zback = [at((z - k + nz) % nz, y, x, c) for k in range(nz)]
     ydev = [at(z, (y + j) % ny, x, c) for j in range(ny)]
     xdev = [at(z, y, (x + i) % nx, c) for i in range(nx)]
-    zorder = near_first(nz)
+    turns = [outward(nz, z, i) for i in range(nz)]
+    zabs = [at(a, y, x, c) for a in turns]
+    far_first = list(range(nz - 1, 0, -1))
 
     barrier = pltpu.get_barrier_semaphore()
     friends = zdev[1:] + ydev[1:] + xdev[1:] + [partner]
@@ -111,7 +116,10 @@
         return up_ref.at[:, pl.ds(pl.multiple_of(to * units, LANES), units)]
 
     def dn_part(to):
-        return dn_ref.at[pl.ds(pl.multiple_of(to * units, LANES), units), :]
+        first = to * units
+        if not isinstance(first, int):
+            first = pl.multiple_of(first, LANES)
+        return dn_ref.at[pl.ds(first, units), :]
 
     local = [
         pltpu.make_async_copy(src, dst, own_sem.at[i])
@@ -134,6 +142,17 @@
     sent = []
     guard = [None]
 
+    def finish(make):
+        remote(*make()).wait_send()
+
+    def drain():
+        for condition, make in sent:
+            if condition is None:
+                finish(make)
+            else:
+                pl.when(condition)(functools.partial(finish, make))
+        sent.clear()
+
     def start(make):
         sent.append((guard[-1], make))
         remote(*make()).start()
@@ -154,19 +173,14 @@
 
     lane = lax.broadcasted_iota(jnp.int32, (tok_rows, LANES), 1)
 
-    def turn(values):
-        swapped = jnp.where(
-            lane < HALF_ROPE,
-            pltpu.roll(values, LANES - HALF_ROPE, 1),
-            pltpu.roll(values, HALF_ROPE, 1),
-        )
-        turned = values * cos_ref[...] + swapped * sin_ref[...]
-        return jnp.where(lane < ROPE_DIM, turned, 0.0)
-
-    spread_ref[...] = jnp.zeros_like(spread_ref)
-    spread_ref[:, :ROPE_DIM] = rope_key[...].astype(jnp.float32)
+    low = rope_t[:HALF_ROPE].astype(jnp.float32)
+    high = rope_t[HALF_ROPE:].astype(jnp.float32)
+    cos, sin = cos_t[...], sin_t[...]
+    stood[...] = jnp.zeros_like(stood)
+    stood[:HALF_ROPE] = low * cos - high * sin
+    stood[HALF_ROPE:ROPE_DIM] = high * cos + low * sin
+    lat_out[s, :, rank:] = stood[...].T.astype(jnp.bfloat16)
     lat_out[s, :, :rank] = rms_scale(kv_lat[...], kv_gain[...]).astype(jnp.bfloat16)
-    lat_out[s, :, rank:] = turn(spread_ref[:, :LANES]).astype(jnp.bfloat16)
 
     with jax.named_scope("greet"):
         pl.semaphore_wait(barrier, len(friends))
@@ -200,44 +214,68 @@
             start(lx(k, j, i, lambda: t))
         start(lc(k, j, 0, c))
 
-    for k in zorder:
+    for k in range(1, nz):
         under(z + k < nz, lambda k=k: start(lz(k, lambda: s)))
     for j in range(1, ny):
         under(y + j < ny, lambda j=j: start(ly(0, j, lambda: s)))
 
-    def z_up(k):
-        return lambda: (up_part((z + k) % nz), up_out.at[s], uz_s.at[k], uz_r.at[k], zdev[k])
-
-    def z_dn(k):
-        return lambda: (dn_part((z + k) % nz), dn_out.at[s], dz_s.at[k], dz_r.at[k], zdev[k])
-
-    for k in zorder:
-        start(z_up(k))
-    for k in zorder:
-        start(z_dn(k))
-    for j in range(1, ny):
-        start(lambda j=j: (up_part(z), up_out.at[s], uy_s.at[0, j], uy_r.at[0, j], ydev[j]))
-
-    def up_forward(k):
-        slot = lambda: up_out.at[block(k, 0)]
-        arrive(lambda: (slot(), slot(), uz_s.at[k], uz_r.at[k], zdev[k]))
+    def z_up(i):
+        a = turns[i]
+        return lambda: (up_part(a), up_out.at[s], uz_s.at[i], uz_r.at[z], zabs[i])
+
+    def z_dn(i):
+        a = turns[i]
+        return lambda: (dn_part(a), dn_out.at[s], dz_s.at[i], dz_r.at[z], zabs[i])
+
+    def forward(i, out, zs, zr, ys, yr):
+        a = turns[i]
+        slot = lambda: out.at[a * ny + y]
+        arrive(lambda: (slot(), slot(), zs.at[i], zr.at[a], zabs[i]))
         for j in range(1, ny):
-            start(lambda j=j: (slot(), slot(), uy_s.at[k, j], uy_r.at[k, j], ydev[j]))
-
-    def dn_forward(k):
-        slot = lambda: dn_out.at[block(k, 0)]
-        arrive(lambda: (slot(), slot(), dz_s.at[k], dz_r.at[k], zdev[k]))
-        for j in range(1, ny):
-            start(lambda j=j: (slot(), slot(), dy_s.at[k, j], dy_r.at[k, j], ydev[j]))
+            start(lambda j=j: (slot(), slot(), ys.at[a, j], yr.at[a, j], ydev[j]))
+
+    def up_forward(i):
+        forward(i, up_out, uz_s, uz_r, uy_s, uy_r)
+
+    def dn_forward(i):
+        forward(i, dn_out, dz_s, dz_r, dy_s, dy_r)
 
     with jax.named_scope("queries"):
-        query_normed = rms_scale(q_lat[...], q_gain[...]).astype(jnp.bfloat16)
+        stood[:HALF_ROPE] = cos
+        stood[HALF_ROPE:ROPE_DIM] = cos
+        cos_ref = stood[...].T
+        stood[:HALF_ROPE] = -sin
+        stood[HALF_ROPE:ROPE_DIM] = sin
+        sin_ref = stood[...].T
+
+        def turn(values):
+            swapped = jnp.where(
+                lane < HALF_ROPE,
+                pltpu.roll(values, LANES - HALF_ROPE, 1),
+                pltpu.roll(values, HALF_ROPE, 1),
+            )
+            turned = values * cos_ref + swapped * sin_ref
+            return jnp.where(lane < ROPE_DIM, turned, 0.0)
+
+        spread_ref[...] = jnp.zeros_like(spread_ref)
+        values = q_lat[...].astype(jnp.float32)
+        values = values * lax.rsqrt(jnp.mean(values * values, axis=-1, keepdims=True) + epsilon)
+        query_normed = jnp.concatenate(
+            [
+                values[:, b * LANES : (b + 1) * LANES] * q_gain[b : b + 1]
+                for b in range(values.shape[1] // LANES)
+            ],
+            axis=1,
+        ).astype(jnp.bfloat16)
         head = 0
         for w_ref, copies, nope in ((wqs, local[0], SMALL_DIM), (wql, local[1], LARGE_DIM)):
             copies.wait()
-            cols = w_ref.shape[1]
-            spread_ref[:, :cols] = jnp.dot(
-                query_normed, w_ref[...], preferred_element_type=jnp.float32
+            cols = w_ref.shape[0]
+            spread_ref[:, :cols] = lax.dot_general(
+                query_normed,
+                w_ref[...],
+                (((1,), (1,)), ((), ())),
+                preferred_element_type=jnp.float32,
             )
 
             def take(first, size):
@@ -331,18 +369,27 @@
             lax.broadcasted_iota(jnp.int32, (tok_rows, tok_rows), 0)
         )
         attend(lat_out[s], ahead, True)
+    with jax.named_scope("drain"):
+        drain()
+        pl.semaphore_signal(go_sem, inc=1, device_id=partner, device_id_type=MESH)
+        pl.semaphore_wait(go_sem, 1)
+    for i in far_first:
+        start(z_up(i))
+    for i in far_first:
+        start(z_dn(i))
+    for j in range(1, ny):
+        start(lambda j=j: (up_part(z), up_out.at[s], uy_s.at[z, j], uy_r.at[z, j], ydev[j]))
     with jax.named_scope("lat_z"):
-        for k in zorder:
+        for k in range(1, nz):
             under(z >= k, lambda k=k: lat_from_z(k))
         for j in range(1, ny):
             under(y >= j, lambda j=j: lat_from_y(0, j))
-    for j in range(1, ny):
-        start(lambda j=j: (dn_part(z), dn_out.at[s], dy_s.at[0, j], dy_r.at[0, j], ydev[j]))
     with jax.named_scope("lat_x0"):
         for j in range(1, ny):
             under(y >= j, lambda j=j: lat_from_x(0, j))
-        for k in zorder:
+        for k in range(1, nz):
             under(z >= k, lambda k=k: lat_from_x(k, 0))
+    with jax.named_scope("lat_c0"):
         for j in range(1, ny):
             under(y >= j, lambda j=j: lat_here(0, j))
     with jax.named_scope("near"):
@@ -352,17 +399,19 @@
 
         lax.fori_loop(0, y, near, 0)
     with jax.named_scope("lat_y"):
-        for k in zorder:
+        for k in range(1, nz):
             for j in range(1, ny):
                 under(z >= k, lambda k=k, j=j: lat_from_y(k, j))
-        for k in zorder:
+        for k in range(1, nz):
             for j in range(1, ny):
                 under(z >= k, lambda k=k, j=j: lat_from_x(k, j))
+    for j in range(1, ny):
+        start(lambda j=j: (dn_part(z), dn_out.at[s], dy_s.at[z, j], dy_r.at[z, j], ydev[j]))
     with jax.named_scope("up_fwd"):
-        for k in zorder[:2]:
-            up_forward(k)
+        for i in far_first[:1]:
+            up_forward(i)
     with jax.named_scope("lat_all"):
-        for k in zorder:
+        for k in range(1, nz):
             for j in range(ny):
                 under(z >= k, lambda k=k, j=j: lat_here(k, j))
     with jax.named_scope("far"):
@@ -412,10 +461,8 @@
             for j in range(1, nx):
                 start(ax(i, j))
     with jax.named_scope("fwd2"):
-        for k in zorder[2:]:
-            up_forward(k)
-        for k in zorder[:2]:
-            dn_forward(k)
+        for i in far_first[1:]:
+            up_forward(i)
     with jax.named_scope("rs_x"):
         for i in range(HALVES):
             mixed = part_ref[i, c, x].astype(jnp.float32)
@@ -426,54 +473,74 @@
             after[:, i * cut : (i + 1) * cut] = piece.astype(jnp.bfloat16)
         xg[z, c, x] = rms_scale(after[...], gain_ref[...]).astype(jnp.bfloat16)
 
-    def bz(k):
-        slot = lambda: xg.at[z, c, x]
-        return lambda: (slot(), slot(), bz_s.at[k], bz_r.at[z], zdev[k])
-
-    def spread(a):
-        slot = lambda: xg.at[a, c, x]
-        for i in range(1, nx):
-            start(lambda i=i: (slot(), slot(), bx_s.at[a, i], bx_r.at[a, i], xdev[i]))
-        start(lambda: (slot(), slot(), bc_s.at[a, 0], bc_r.at[a, 0], partner))
-
-    for k in zorder:
-        start(bz(k))
-    spread(z)
-    with jax.named_scope("fwd3"):
-        for k in zorder[2:]:
-            dn_forward(k)
-    with jax.named_scope("g_z"):
-        for a in range(nz):
-            def from_z(a=a):
-                slot = lambda: xg.at[a, c, x]
-                arrive(lambda: (slot(), slot(), bz_s.at[0], bz_r.at[a], partner))
-                for i in range(1, nx):
-                    start(lambda i=i: (slot(), slot(), bx_s.at[a, i], bx_r.at[a, i], xdev[i]))
-                start(lambda: (slot(), slot(), bc_s.at[a, 0], bc_r.at[a, 0], partner))
-
-            under(z != a, from_z)
+    piece_rows = rows // HALVES
 
     def xi(i):
         return (x - i + nx) % nx
 
-    def from_x(a):
+    def piece(a, cc, xx, h):
+        return xg.at[a, cc, xx, pl.ds(h * piece_rows, piece_rows)]
+
+    def hop(a, h, send_sem, to):
+        return lambda: (
+            piece(a, c, x, h), piece(a, c, x, h), send_sem(), bz_r.at[a, h], at(to(), y, x, c)
+        )
+
+    def bx(a, i, h, xx):
+        return lambda: (
+            piece(a, c, xx(i), h), piece(a, c, xx(i), h), bx_s.at[a, i, h], bx_r.at[a, i, h], xdev[i]
+        )
+
+    def bc(a, i, h, cc):
+        return lambda: (
+            piece(a, cc, xi(i), h), piece(a, cc, xi(i), h),
+            bc_s.at[a, i, h], bc_r.at[a, i, h], partner,
+        )
+
+    def own_x(i):
+        return x
+
+    def spread(a, h):
         for i in range(1, nx):
-            slot = lambda i=i: xg.at[a, c, xi(i)]
-            arrive(lambda: (slot(), slot(), bx_s.at[a, i], bx_r.at[a, i], xdev[i]))
-            start(lambda i=i, slot=slot: (slot(), slot(), bc_s.at[a, i], bc_r.at[a, i], partner))
+            start(bx(a, i, h, own_x))
+        start(bc(a, 0, h, c))
+
+    for h in range(HALVES):
+        under(z + 1 < nz, lambda h=h: start(hop(z, h, lambda: bz_s.at[z, h], lambda: z + 1)))
+        under(z > 0, lambda h=h: start(hop(z, h, lambda: bo_s.at[h], lambda: z - 1)))
+        spread(z, h)
+
+    def from_z(i):
+        a = turns[i]
+        after_me = z + 2 * jnp.minimum(jnp.maximum(z - a, 0), 1) - 1
+        onward = (after_me >= 0) & (after_me < nz)
+        for h in range(HALVES):
+            arrive(hop(a, h, lambda: bz_s.at[a, h], lambda: z))
+            under(
+                onward, lambda h=h: start(hop(a, h, lambda: bz_s.at[a, h], lambda: after_me))
+            )
+            spread(a, h)
+
+    def from_x(i):
+        a = turns[i]
+        for h in range(HALVES):
+            for j in range(1, nx):
+                arrive(bx(a, j, h, xi))
+                start(bc(a, j, h, c))
 
     def rows_here(a):
-        for i in range(nx):
-            slot = lambda i=i: xg.at[a, 1 - c, xi(i)]
-            arrive(lambda: (slot(), slot(), bc_s.at[a, i], bc_r.at[a, i], partner))
+        for h in range(HALVES):
+            for j in range(nx):
+                arrive(bc(a, j, h, 1 - c))
 
     def weights_here(out, sy, ry):
-        for k in range(nz):
+        for a in range(nz):
             for j in range(1, ny):
-                slot = lambda: out.at[block(k, j)]
-                arrive(lambda: (slot(), slot(), sy.at[k, j], ry.at[k, j], ydev[j]))
-
-    def up_step(a):
+                slot = lambda: out.at[a * ny + (y - j + ny) % ny]
+                arrive(lambda: (slot(), slot(), sy.at[a, j], ry.at[a, j], ydev[j]))
+
+    def up_step(i):
+        a = turns[i]
         rows_here(a)
         tokens = xg[a].reshape(tp * rows, width)
         projected = jnp.dot(
@@ -482,7 +549,7 @@
         hid[a] = jnp.square(jnp.maximum(projected, 0.0)).astype(jnp.bfloat16)
 
     def down_step(k):
-        hidden = hid[zi(k)]
+        hidden = hid[turns[k]]
         cols = dn_out.shape[2]
         for b in range(dn_out.shape[0]):
             out = jnp.dot(hidden, dn_out[b], preferred_element_type=jnp.float32)
@@ -510,49 +577,71 @@
             summed = summed + xbuf[k, j].astype(jnp.float32)
         zsend[k] = summed.astype(jnp.bfloat16)
         if k:
-            start(lambda: (zsend.at[k], zbuf.at[k], cz_s.at[k], cz_r.at[k], zback[k]))
-
+            start(lambda: (zsend.at[k], zbuf.at[z], cz_s.at[k], cz_r.at[z], zabs[k]))
+
+    with jax.named_scope("fwd3"):
+        dn_forward(nz - 1)
     with jax.named_scope("g_x"):
         from_x(0)
+    if nz > 2:
+        with jax.named_scope("g_z"):
+            from_z(1)
+    with jax.named_scope("fwd4"):
+        for i in far_first[1:]:
+            dn_forward(i)
     local[6].wait()
+    local[7].wait()
     with jax.named_scope("w_up"):
         weights_here(up_out, uy_s, uy_r)
-    for a in range(nz):
-        if a + 1 < nz:
-            with jax.named_scope("g_x"):
-                from_x(a + 1)
+    with jax.named_scope("up"):
+        up_step(0)
+    for i in range(1, nz - 1):
+        with jax.named_scope("g_x"):
+            from_x(i)
+        if i + 1 < nz - 1:
+            with jax.named_scope("g_z"):
+                from_z(i + 1)
         with jax.named_scope("up"):
-            up_step(a)
-    local[7].wait()
+            up_step(i)
+    late = [nz - 1] if nz > 1 else []
+    for i in late:
+        with jax.named_scope("g_z"):
+            from_z(i)
     with jax.named_scope("w_dn"):
         weights_here(dn_out, dy_s, dy_r)
-    order = zorder[::-1] + [0]
+    order = list(range(nz - 2, 0, -1)) + late + [0]
+    for i in order[:-2]:
+        with jax.named_scope("down"):
+            down_step(i)
+    with jax.named_scope("core"):
+        for i in order[:-2]:
+            core_sum(i)
+    for i in late:
+        with jax.named_scope("g_x"):
+            from_x(i)
+        with jax.named_scope("up"):
+            up_step(i)
+        with jax.named_scope("down"):
+            down_step(i)
     with jax.named_scope("down"):
-        for i, k in enumerate(order):
-            down_step(k)
-            if i:
-                core_sum(order[i - 1])
-        core_sum(order[-1])
-    for k in order:
+        down_step(0)
+    with jax.named_scope("core"):
+        for i in late + [0]:
+            core_sum(i)
+    for i in order:
         with jax.named_scope("cross"):
-            cross_sum(k)
+            cross_sum(i)
     with jax.named_scope("final"):
         final = after[...].astype(jnp.float32)
         ffn = zsend[0].astype(jnp.float32)
-        for k in order[:-1]:
-            arrive(lambda: (zbuf.at[k], zbuf.at[k], cz_s.at[k], cz_r.at[k], zback[k]))
-            ffn = ffn + zbuf[k].astype(jnp.float32)
+        for k in range(1, nz):
+            a = turns[k]
+            arrive(lambda: (zbuf.at[a], zbuf.at[a], cz_s.at[k], cz_r.at[a], zabs[k]))
+            ffn = ffn + zbuf[a].astype(jnp.float32)
         out_ref[...] = (final + ffn).astype(jnp.bfloat16)
 
-    def finish(make):
-        remote(*make()).wait_send()
-
     with jax.named_scope("wait_send"):
-        for condition, make in sent:
-            if condition is None:
-                finish(make)
-            else:
-                pl.when(condition)(functools.partial(finish, make))
+        drain()
 
 
 def layer(
@@ -566,7 +655,7 @@
     large = wkl.shape[1] // (2 * LARGE_DIM)
     heads = small + large
     units = w_up.shape[1] // nz
-    query_cols = -(-max(wqs.shape[1], wql.shape[1]) // LANES) * LANES
+    query_cols = -(-max(wqs.shape[0], wql.shape[0]) // LANES) * LANES
     dma = pltpu.SemaphoreType.DMA
     vmem = pl.BlockSpec(memory_space=pltpu.VMEM)
     anywhere = pl.BlockSpec(memory_space=pl.ANY)
@@ -593,6 +682,7 @@
             like(wkl),
             like(wos),
             like(wol),
+            pltpu.VMEM((LANES, tok_rows), f32),
             pltpu.VMEM((tok_rows, query_cols), f32),
             pltpu.VMEM((heads, tok_rows, 2 * LANES), b16),
             pltpu.VMEM((heads, tok_rows, 1), f32),
@@ -610,6 +700,7 @@
             pltpu.VMEM((nz, rows, width), b16),
             pltpu.VMEM((nz, rows, width), b16),
             dma((8,)),
+            pltpu.SemaphoreType.REGULAR,
         ]
         + pair(nz)
         + pair(nz, ny)
@@ -617,8 +708,9 @@
         + (pair(nz) + pair(nz, ny)) * 2
         + pair(HALVES)
         + pair(HALVES, nx)
-        + pair(nz)
-        + pair(nz, nx) * 2
+        + pair(nz, HALVES)
+        + [dma((HALVES,))]
+        + pair(nz, nx, HALVES) * 2
         + pair(nz)
         + pair(nz, nx)
         + pair(nz),
@@ -661,15 +753,15 @@
         nx,
         q_latent,
         kv_latent,
-        rope_key,
+        rope_key.T,
         cos,
         sin,
-        q_gain.reshape(1, -1),
+        q_gain.reshape(-1, LANES),
         kv_gain.reshape(1, -1),
         ffn_gain.reshape(1, -1),
         resid,
-        w_q_small,
-        w_q_large,
+        w_q_small.T,
+        w_q_large.T,
         w_kv_small,
         w_kv_large,
         w_out_small,

time: 134 us -> 120 us (0.90)
  the two profiles are of different devices: /device:TPU:15 before, /device:TPU:0 now
where the time goes in v2:
time: 120 us
  Pallas kernels  118 us (98%)
  local copies, waits for them, and re-layouts  1.67 us (1%)
    pallas_call x1, Pallas kernels, layer(): pl.pallas_call(functools.partial(layer_kernel, ny, nz, nx), out_shape=jax...  118 us

profile of v2, /device:TPU:0, one launch (start us, length us, event | category | flops | bytes accessed | tf_op | source)
XLA Modules:
  0.0 120.2 jit_solution(12658394948227195654)
XLA Ops:
  0.0 0.8 multiply_sine_fusion
  0.8 117.8 %layer.1 = bf16[64,2048]{1,0:T(8,128)(2,1)} custom-call(bf16[256,768]{1,0:T(8,128)(2,1)} %q_lat.1, bf16[256,512]{1,0:T(8,128)(2,1)} %kv_lat.1, bf16[32,256]{1,0:T(8,128)(2,1)} %bitcast.8, f32[16,256]{1,0:T(8,128)} %get-tuple-element.6.cos_t, f32[16,256]{1,0:T(8,128)} %get-tuple-element.5.sin_t, f32[6,128]{1,0:T(8,128)} %bitcast.10, f32[1,512]{1,0:T(1,128)} %bitcast.11, ...), custom_call_target="tpu_custom_call" | custom-call | tf_op jit(solution)/shard_map/layer/pallas_call | solution.py:670
  118.6 1.7 %copy.17 = bf16[64,2048]{1,0:T(8,128)(2,1)} copy(bf16[64,2048]{1,0:T(8,128)(2,1)} %layer.1) | data formatting | bytes 524288
  (2 shorter events, 0.0 us)

commit v3 on v2

--- a/solution.py
+++ b/solution.py
@@ -82,11 +82,11 @@
     wqs_hbm, wql_hbm, wks_hbm, wkl_hbm, wos_hbm, wol_hbm, up_ref, dn_ref, out_ref,
     lat_out, up_out, dn_out, wqs, wql, wks, wkl, wos, wol, stood, spread_ref, q_all,
     row_max, row_sum, weighted, part_ref, rs_c, rs_x, after, xg, hid,
-    pbuf, cbuf, xbuf, zsend, zbuf, own_sem, go_sem,
+    pbuf, cbuf, xbuf, zsend, zbuf, ebuf, own_sem, go_sem,
     lz_s, lz_r, ly_s, ly_r, lx_s, lx_r, lc_s, lc_r,
     uz_s, uz_r, uy_s, uy_r, dz_s, dz_r, dy_s, dy_r,
     ac_s, ac_r, ax_s, ax_r, bz_s, bz_r, bo_s, bx_s, bx_r, bc_s, bc_r,
-    cc_s, cc_r, cx_s, cx_r, cz_s, cz_r,
+    cc_s, cc_r, cx_s, cx_r, cz_s, cz_r, ez_r,
 ):
     z, y, x, c, at = place(ny, nz, nx)
     s = z * ny + y
@@ -510,15 +510,18 @@
         under(z > 0, lambda h=h: start(hop(z, h, lambda: bo_s.at[h], lambda: z - 1)))
         spread(z, h)
 
-    def from_z(i):
+    after_me = [z + 2 * jnp.minimum(jnp.maximum(z - a, 0), 1) - 1 for a in turns]
+    onward = [(a >= 0) & (a < nz) for a in after_me]
+
+    def from_z(i, relay=True):
         a = turns[i]
-        after_me = z + 2 * jnp.minimum(jnp.maximum(z - a, 0), 1) - 1
-        onward = (after_me >= 0) & (after_me < nz)
         for h in range(HALVES):
             arrive(hop(a, h, lambda: bz_s.at[a, h], lambda: z))
-            under(
-                onward, lambda h=h: start(hop(a, h, lambda: bz_s.at[a, h], lambda: after_me))
-            )
+            if relay:
+                under(
+                    onward[i],
+                    lambda h=h: start(hop(a, h, lambda: bz_s.at[a, h], lambda: after_me[i])),
+                )
             spread(a, h)
 
     def from_x(i):
@@ -533,11 +536,11 @@
             for j in range(nx):
                 arrive(bc(a, j, h, 1 - c))
 
-    def weights_here(out, sy, ry):
-        for a in range(nz):
-            for j in range(1, ny):
-                slot = lambda: out.at[a * ny + (y - j + ny) % ny]
-                arrive(lambda: (slot(), slot(), sy.at[a, j], ry.at[a, j], ydev[j]))
+    def from_y(p, out, sy, ry):
+        a = turns[p]
+        for j in range(1, ny):
+            slot = lambda: out.at[a * ny + (y - j + ny) % ny]
+            arrive(lambda: (slot(), slot(), sy.at[a, j], ry.at[a, j], ydev[j]))
 
     def up_step(i):
         a = turns[i]
@@ -548,36 +551,98 @@
         )
         hid[a] = jnp.square(jnp.maximum(projected, 0.0)).astype(jnp.bfloat16)
 
-    def down_step(k):
-        hidden = hid[turns[k]]
+    to_core, to_cross = [], []
+    at_end = (z == 0) | (z == nz - 1)
+    inside = jnp.logical_not(at_end)
+    takes = [((z == 1) & (a > z)) | ((z == nz - 2) & (a < z)) for a in turns]
+    takes = [inside & yes for yes in takes]
+    alone = [inside & jnp.logical_not(yes) for yes in takes]
+    apart = [
+        ((a == 0) | (a == nz - 1)) & ((a - z > 1) | (z - a > 1)) for a in turns
+    ]
+
+    def inward(i, p):
+        return lambda: (
+            zsend.at[i, p], ebuf.at[turns[i], turns[p]],
+            cz_s.at[i, p], ez_r.at[turns[i], turns[p]], zabs[1],
+        )
+
+    def outward_sum(i, p):
+        return lambda: (
+            zsend.at[i, p], zbuf.at[z, turns[p]],
+            cz_s.at[i, p], cz_r.at[z, turns[p]], zabs[i],
+        )
+
+    def core_send(i, p):
+        return lambda: (
+            pbuf.at[i, p, 1 - c], cbuf.at[i, p], cc_s.at[i, p], cc_r.at[i, p], partner
+        )
+
+    def cross_send(i, p, j):
+        return lambda: (
+            pbuf.at[i, p, c, (x + j) % nx], xbuf.at[i, p, j],
+            cx_s.at[i, p, j], cx_r.at[i, p, j], xdev[j],
+        )
+
+    def down_step(i, p):
+        hidden = hid[turns[i]]
         cols = dn_out.shape[2]
-        for b in range(dn_out.shape[0]):
-            out = jnp.dot(hidden, dn_out[b], preferred_element_type=jnp.float32)
-            pbuf[k, :, :, :, b * cols : (b + 1) * cols] = out.astype(jnp.bfloat16).reshape(
+        for j in range(ny):
+            out = jnp.dot(hidden, dn_out[turns[p] * ny + j], preferred_element_type=jnp.float32)
+            pbuf[i, p, :, :, :, j * cols : (j + 1) * cols] = out.astype(jnp.bfloat16).reshape(
                 CORES, nx, rows, cols
             )
-        start(lambda: (pbuf.at[k, 1 - c], cbuf.at[k], cc_s.at[k], cc_r.at[k], partner))
-
-    def core_sum(k):
-        arrive(lambda: (cbuf.at[k], cbuf.at[k], cc_s.at[k], cc_r.at[k], partner))
-        pbuf[k, c] = (
-            pbuf[k, c].astype(jnp.float32) + cbuf[k].astype(jnp.float32)
+        start(core_send(i, p))
+
+    def core_sum(i, p):
+        arrive(core_send(i, p))
+        pbuf[i, p, c] = (
+            pbuf[i, p, c].astype(jnp.float32) + cbuf[i, p].astype(jnp.float32)
         ).astype(jnp.bfloat16)
         for j in range(1, nx):
-            start(
-                lambda j=j: (
-                    pbuf.at[k, c, (x + j) % nx], xbuf.at[k, j], cx_s.at[k, j], cx_r.at[k, j], xdev[j]
-                )
-            )
-
-    def cross_sum(k):
-        summed = pbuf[k, c, x].astype(jnp.float32)
+            start(cross_send(i, p, j))
+
+    def cross_sum(i, p):
+        summed = pbuf[i, p, c, x].astype(jnp.float32)
         for j in range(1, nx):
-            arrive(lambda: (xbuf.at[k, j], xbuf.at[k, j], cx_s.at[k, j], cx_r.at[k, j], xdev[j]))
-            summed = summed + xbuf[k, j].astype(jnp.float32)
-        zsend[k] = summed.astype(jnp.bfloat16)
-        if k:
-            start(lambda: (zsend.at[k], zbuf.at[z], cz_s.at[k], cz_r.at[z], zabs[k]))
+            arrive(cross_send(i, p, j))
+            summed = summed + xbuf[i, p, j].astype(jnp.float32)
+        summed = summed.astype(jnp.bfloat16)
+        if i > 1:
+            zsend[i, p] = summed
+            under(at_end, lambda: start(inward(i, p)))
+            under(alone[i], lambda: start(outward_sum(i, p)))
+        elif i:
+            zsend[i, p] = summed
+            start(outward_sum(i, p))
+        else:
+            zbuf[z, turns[p]] = summed
+
+    def combine(i, p):
+        def add():
+            arrive(inward(i, p))
+            zsend[i, p] = (
+                zsend[i, p].astype(jnp.float32)
+                + ebuf[turns[i], turns[p]].astype(jnp.float32)
+            ).astype(jnp.bfloat16)
+            start(outward_sum(i, p))
+
+        under(takes[i], add)
+
+    def advance(core_lag, cross_lag):
+        while len(to_core) > core_lag:
+            job = to_core.pop(0)
+            core_sum(*job)
+            to_cross.append(job)
+        while len(to_cross) > cross_lag:
+            cross_sum(*to_cross.pop(0))
+
+    def jobs(these):
+        for job in these:
+            down_step(*job)
+            to_core.append(job)
+            advance(2, 5)
+        advance(0, 5)
 
     with jax.named_scope("fwd3"):
         dn_forward(nz - 1)
@@ -586,59 +651,90 @@
     if nz > 2:
         with jax.named_scope("g_z"):
             from_z(1)
+    for i in range(2, nz - 1):
+        with jax.named_scope("g_z"):
+            under(inside, lambda i=i: from_z(i))
     with jax.named_scope("fwd4"):
         for i in far_first[1:]:
             dn_forward(i)
+    late = [nz - 1] if nz > 1 else []
     local[6].wait()
     local[7].wait()
     with jax.named_scope("w_up"):
-        weights_here(up_out, uy_s, uy_r)
+        for p in range(nz):
+            from_y(p, up_out, uy_s, uy_r)
     with jax.named_scope("up"):
         up_step(0)
+    first_in = [0] + late
+    rest = list(range(nz - 2, 0, -1))
+    with jax.named_scope("w_dn0"):
+        for p in first_in:
+            from_y(p, dn_out, dy_s, dy_r)
+    with jax.named_scope("jobs"):
+        jobs([(0, p) for p in first_in])
     for i in range(1, nz - 1):
         with jax.named_scope("g_x"):
             from_x(i)
-        if i + 1 < nz - 1:
+        if i == nz - 2:
             with jax.named_scope("g_z"):
-                from_z(i + 1)
+                under(at_end, lambda i=i: from_z(i + 1, False))
         with jax.named_scope("up"):
             up_step(i)
-    late = [nz - 1] if nz > 1 else []
-    for i in late:
-        with jax.named_scope("g_z"):
-            from_z(i)
-    with jax.named_scope("w_dn"):
-        weights_here(dn_out, dy_s, dy_r)
-    order = list(range(nz - 2, 0, -1)) + late + [0]
-    for i in order[:-2]:
-        with jax.named_scope("down"):
-            down_step(i)
-    with jax.named_scope("core"):
-        for i in order[:-2]:
-            core_sum(i)
+        with jax.named_scope("jobs"):
+            jobs([(i, p) for p in first_in])
+        if i < nz - 2:
+            with jax.named_scope("g_z"):
+                under(at_end, lambda i=i: from_z(i + 1, False))
+        if i == 1:
+            for n in late:
+                with jax.named_scope("g_z"):
+                    under(inside, lambda n=n: from_z(n))
+            with jax.named_scope("w_dn"):
+                for p in rest:
+                    from_y(p, dn_out, dy_s, dy_r)
+        with jax.named_scope("jobs"):
+            jobs([(i, p) for p in rest])
     for i in late:
         with jax.named_scope("g_x"):
             from_x(i)
         with jax.named_scope("up"):
             up_step(i)
-        with jax.named_scope("down"):
-            down_step(i)
-    with jax.named_scope("down"):
-        down_step(0)
-    with jax.named_scope("core"):
-        for i in late + [0]:
-            core_sum(i)
-    for i in order:
-        with jax.named_scope("cross"):
-            cross_sum(i)
+        with jax.named_scope("jobs"):
+            jobs([(i, p) for p in first_in + rest])
+    outer_order = [1] + list(range(nz - 1, 1, -1)) + [0]
+    with jax.named_scope("jobs"):
+        jobs([(0, p) for p in rest])
+    waiting = [(i, p) for i in range(2, nz - 1) for p in outer_order]
+    with jax.named_scope("cross"):
+        while to_cross:
+            advance(0, len(to_cross) - 1)
+            if waiting:
+                combine(*waiting.pop(0))
+        for pair in waiting:
+            combine(*pair)
+    with jax.named_scope("comb3"):
+        for i in range(max(nz - 1, 2), nz):
+            for p in outer_order:
+                combine(i, p)
     with jax.named_scope("final"):
-        final = after[...].astype(jnp.float32)
-        ffn = zsend[0].astype(jnp.float32)
-        for k in range(1, nz):
-            a = turns[k]
-            arrive(lambda: (zbuf.at[a], zbuf.at[a], cz_s.at[k], cz_r.at[a], zabs[k]))
-            ffn = ffn + zbuf[a].astype(jnp.float32)
-        out_ref[...] = (final + ffn).astype(jnp.bfloat16)
+        group = zbuf.shape[3]
+        for p in range(nz):
+            for k in range(1, nz):
+                slot = lambda: zbuf.at[turns[k], p]
+                make = lambda: (slot(), slot(), cz_s.at[k, p], cz_r.at[turns[k], p], zabs[k])
+                if k == 1:
+                    arrive(make)
+                    continue
+
+                def nothing():
+                    zbuf[turns[k], p] = jnp.zeros(zbuf.shape[2:], zbuf.dtype)
+
+                pl.when(apart[k])(nothing)
+                pl.when(jnp.logical_not(apart[k]))(lambda: arrive(make))
+            ffn = after[:, p * group : (p + 1) * group].astype(jnp.float32)
+            for a in range(nz):
+                ffn = ffn + zbuf[a, p].astype(jnp.float32)
+            out_ref[:, p * group : (p + 1) * group] = ffn.astype(jnp.bfloat16)
 
     with jax.named_scope("wait_send"):
         drain()
@@ -694,11 +790,12 @@
             pltpu.VMEM((rows, width), b16),
             pltpu.VMEM((nz, CORES, nx, rows, width), b16),
             pltpu.VMEM((nz, tp * rows, units), b16),
-            pltpu.VMEM((nz, CORES, nx, rows, width), b16),
-            pltpu.VMEM((nz, nx, rows, width), b16),
-            pltpu.VMEM((nz, nx, rows, width), b16),
-            pltpu.VMEM((nz, rows, width), b16),
-            pltpu.VMEM((nz, rows, width), b16),
+            pltpu.VMEM((nz, nz, CORES, nx, rows, width // nz), b16),
+            pltpu.VMEM((nz, nz, nx, rows, width // nz), b16),
+            pltpu.VMEM((nz, nz, nx, rows, width // nz), b16),
+            pltpu.VMEM((nz, nz, rows, width // nz), b16),
+            pltpu.VMEM((nz, nz, rows, width // nz), b16),
+            pltpu.VMEM((nz, nz, rows, width // nz), b16),
             dma((8,)),
             pltpu.SemaphoreType.REGULAR,
         ]
@@ -711,9 +808,10 @@
         + pair(nz, HALVES)
         + [dma((HALVES,))]
         + pair(nz, nx, HALVES) * 2
-        + pair(nz)
-        + pair(nz, nx)
-        + pair(nz),
+        + pair(nz, nz)
+        + pair(nz, nz, nx)
+        + pair(nz, nz)
+        + [dma((nz, nz))],
         compiler_params=pltpu.CompilerParams(
             collective_id=1, has_side_effects=True, vmem_limit_bytes=63 * 2**20
         ),

time: 120 us -> 116 us (0.967)
  Pallas kernels: 118 us -> 113 us
    pallas_call x1, Pallas kernels: 118 us -> 113 us  [layer(): pl.pallas_call(functools.partial(layer_kernel, ny, nz, nx), out_shape=jax...]
where the time goes in v3:
time: 116 us; the launch traced here: 115 us
  Pallas kernels  113 us (97%)
  local copies, waits for them, and re-layouts  1.67 us (1%)
    pallas_call x1, Pallas kernels, layer(): pl.pallas_call(functools.partial(layer_kernel, ny, nz, nx), out_shape=jax...  113 us

profile of v3, /device:TPU:0, one launch (start us, length us, event | category | flops | bytes accessed | tf_op | source)
XLA Modules:
  0.0 115.4 jit_solution(2675590631698673075)
XLA Ops:
  0.0 0.8 multiply_sine_fusion
  0.8 113.0 %layer.1 = bf16[64,2048]{1,0:T(8,128)(2,1)} custom-call(bf16[256,768]{1,0:T(8,128)(2,1)} %q_lat.1, bf16[256,512]{1,0:T(8,128)(2,1)} %kv_lat.1, bf16[32,256]{1,0:T(8,128)(2,1)} %bitcast.8, f32[16,256]{1,0:T(8,128)} %get-tuple-element.6.cos_t, f32[16,256]{1,0:T(8,128)} %get-tuple-element.5.sin_t, f32[6,128]{1,0:T(8,128)} %bitcast.10, f32[1,512]{1,0:T(1,128)} %bitcast.11, ...), custom_call_target="tpu_custom_call" | custom-call | tf_op jit(solution)/shard_map/layer/pallas_call | solution.py:766
  113.7 1.7 %copy.17 = bf16[64,2048]{1,0:T(8,128)(2,1)} copy(bf16[64,2048]{1,0:T(8,128)(2,1)} %layer.1) | data formatting | bytes 524288
  (2 shorter events, 0.0 us)

commit v4 on v3

--- a/solution.py
+++ b/solution.py
@@ -375,8 +375,10 @@
         pl.semaphore_wait(go_sem, 1)
     for i in far_first:
         start(z_up(i))
+    at_end = (z == 0) | (z == nz - 1)
+    inside = jnp.logical_not(at_end)
     for i in far_first:
-        start(z_dn(i))
+        under(at_end, lambda i=i: start(z_dn(i)))
     for j in range(1, ny):
         start(lambda j=j: (up_part(z), up_out.at[s], uy_s.at[z, j], uy_r.at[z, j], ydev[j]))
     with jax.named_scope("lat_z"):
@@ -460,8 +462,8 @@
             ).astype(jnp.bfloat16)
             for j in range(1, nx):
                 start(ax(i, j))
-    with jax.named_scope("fwd2"):
-        for i in far_first[1:]:
+    with jax.named_scope("fwd1"):
+        for i in far_first[1:][-1:]:
             up_forward(i)
     with jax.named_scope("rs_x"):
         for i in range(HALVES):
@@ -509,6 +511,13 @@
         under(z + 1 < nz, lambda h=h: start(hop(z, h, lambda: bz_s.at[z, h], lambda: z + 1)))
         under(z > 0, lambda h=h: start(hop(z, h, lambda: bo_s.at[h], lambda: z - 1)))
         spread(z, h)
+    lower_inside = inside & (2 * z < nz)
+    upper_inside = inside & (2 * z >= nz)
+    for i in far_first:
+        under(inside if i != 2 else lower_inside, lambda i=i: start(z_dn(i)))
+    with jax.named_scope("fwd2"):
+        for i in far_first[1:-1]:
+            up_forward(i)
 
     after_me = [z + 2 * jnp.minimum(jnp.maximum(z - a, 0), 1) - 1 for a in turns]
     onward = [(a >= 0) & (a < nz) for a in after_me]
@@ -552,8 +561,6 @@
         hid[a] = jnp.square(jnp.maximum(projected, 0.0)).astype(jnp.bfloat16)
 
     to_core, to_cross = [], []
-    at_end = (z == 0) | (z == nz - 1)
-    inside = jnp.logical_not(at_end)
     takes = [((z == 1) & (a > z)) | ((z == nz - 2) & (a < z)) for a in turns]
     takes = [inside & yes for yes in takes]
     alone = [inside & jnp.logical_not(yes) for yes in takes]
@@ -641,8 +648,8 @@
         for job in these:
             down_step(*job)
             to_core.append(job)
-            advance(2, 5)
-        advance(0, 5)
+            advance(2, 6)
+        advance(0, 6)
 
     with jax.named_scope("fwd3"):
         dn_forward(nz - 1)
@@ -651,13 +658,13 @@
     if nz > 2:
         with jax.named_scope("g_z"):
             from_z(1)
+        under(upper_inside, lambda: start(z_dn(2)))
+    late = [nz - 1] if nz > 1 else []
+    first_in = [0] + late
+    rest = list(range(nz - 2, 0, -1))
     for i in range(2, nz - 1):
         with jax.named_scope("g_z"):
             under(inside, lambda i=i: from_z(i))
-    with jax.named_scope("fwd4"):
-        for i in far_first[1:]:
-            dn_forward(i)
-    late = [nz - 1] if nz > 1 else []
     local[6].wait()
     local[7].wait()
     with jax.named_scope("w_up"):
@@ -665,35 +672,37 @@
             from_y(p, up_out, uy_s, uy_r)
     with jax.named_scope("up"):
         up_step(0)
-    first_in = [0] + late
-    rest = list(range(nz - 2, 0, -1))
+    for i in range(1, min(2, nz - 1)):
+        with jax.named_scope("g_x"):
+            from_x(i)
+        with jax.named_scope("up"):
+            up_step(i)
     with jax.named_scope("w_dn0"):
         for p in first_in:
             from_y(p, dn_out, dy_s, dy_r)
     with jax.named_scope("jobs"):
-        jobs([(0, p) for p in first_in])
-    for i in range(1, nz - 1):
+        jobs([(i, p) for i in range(min(2, nz - 1)) for p in first_in])
+    for i in late:
+        with jax.named_scope("g_z"):
+            under(inside, lambda i=i: from_z(i))
+    with jax.named_scope("fwd4"):
+        for i in far_first[1:]:
+            dn_forward(i)
+    for i in range(2, nz):
+        with jax.named_scope("g_z"):
+            under(at_end, lambda i=i: from_z(i, False))
+    for i in range(2, nz - 1):
         with jax.named_scope("g_x"):
             from_x(i)
-        if i == nz - 2:
-            with jax.named_scope("g_z"):
-                under(at_end, lambda i=i: from_z(i + 1, False))
         with jax.named_scope("up"):
             up_step(i)
         with jax.named_scope("jobs"):
             jobs([(i, p) for p in first_in])
-        if i < nz - 2:
-            with jax.named_scope("g_z"):
-                under(at_end, lambda i=i: from_z(i + 1, False))
-        if i == 1:
-            for n in late:
-                with jax.named_scope("g_z"):
-                    under(inside, lambda n=n: from_z(n))
-            with jax.named_scope("w_dn"):
-                for p in rest:
-                    from_y(p, dn_out, dy_s, dy_r)
+    for p in rest:
+        with jax.named_scope("w_dn"):
+            from_y(p, dn_out, dy_s, dy_r)
         with jax.named_scope("jobs"):
-            jobs([(i, p) for p in rest])
+            jobs([(i, p) for i in range(nz - 2, 0, -1)])
     for i in late:
         with jax.named_scope("g_x"):
             from_x(i)
@@ -706,7 +715,8 @@
         jobs([(0, p) for p in rest])
     waiting = [(i, p) for i in range(2, nz - 1) for p in outer_order]
     with jax.named_scope("cross"):
-        while to_cross:
+        own_jobs = len([1 for job in to_cross if job[0] == 0])
+        while len(to_cross) > own_jobs:
             advance(0, len(to_cross) - 1)
             if waiting:
                 combine(*waiting.pop(0))
@@ -716,6 +726,8 @@
         for i in range(max(nz - 1, 2), nz):
             for p in outer_order:
                 combine(i, p)
+    with jax.named_scope("cross_own"):
+        advance(0, 0)
     with jax.named_scope("final"):
         group = zbuf.shape[3]
         for p in range(nz):

time: 116 us -> 115 us (level)
    pallas_call x1, Pallas kernels: 113 us -> 112 us  [layer(): pl.pallas_call(functools.partial(layer_kernel, ny, nz, nx), out_shape=jax...]
where the time goes in v4:
time: 115 us; the launch traced here: 114 us
  Pallas kernels  112 us (97%)
  local copies, waits for them, and re-layouts  1.67 us (1%)
    pallas_call x1, Pallas kernels, layer(): pl.pallas_call(functools.partial(layer_kernel, ny, nz, nx), out_shape=jax...  112 us

profile of v4, /device:TPU:0, one launch (start us, length us, event | category | flops | bytes accessed | tf_op | source)
XLA Modules:
  0.0 114.2 jit_solution(5127050822550294419)
XLA Ops:
  0.0 0.8 multiply_sine_fusion
  0.8 111.7 %layer.1 = bf16[64,2048]{1,0:T(8,128)(2,1)} custom-call(bf16[256,768]{1,0:T(8,128)(2,1)} %q_lat.1, bf16[256,512]{1,0:T(8,128)(2,1)} %kv_lat.1, bf16[32,256]{1,0:T(8,128)(2,1)} %bitcast.8, f32[16,256]{1,0:T(8,128)} %get-tuple-element.6.cos_t, f32[16,256]{1,0:T(8,128)} %get-tuple-element.5.sin_t, f32[6,128]{1,0:T(8,128)} %bitcast.10, f32[1,512]{1,0:T(1,128)} %bitcast.11, ...), custom_call_target="tpu_custom_call" | custom-call | tf_op jit(solution)/shard_map/layer/pallas_call | solution.py:778
  112.5 1.7 %copy.17 = bf16[64,2048]{1,0:T(8,128)(2,1)} copy(bf16[64,2048]{1,0:T(8,128)(2,1)} %layer.1) | data formatting | bytes 524288
  (2 shorter events, 0.0 us)
